TPU v7x, 32 devices: a whole 2x2x4 slice. The times are simulated.
32 devices in a mesh: sp: 8 (over z, x), tp: 4 (over y, core).
Axes of the slice: x: 2, y: 2, z: 4, core: 2. Of those that a mesh axis runs over, the one named last changes fastest.
Arguments:
- query_maps: bfloat16 [1536, 1024], P('sp', 'tp'), may hold values from -6 to 6
- key_maps: bfloat16 [1536, 512], P('sp', 'tp'), may hold values from -6 to 6
- value_rows: bfloat16 [1536, 512], P('sp', 'tp'), may hold values from -6 to 6
- mix_lambda: float32 [8], P('tp'), may hold values from 0.3 to 0.8
- head_gain: float32 [128], replicated, may hold values from 0.1 to 1.9
- out_weight: bfloat16 [1024, 2048], replicated, may hold values from -0.1875 to 0.1875
- residual: bfloat16 [1536, 2048], P(('sp', 'tp')), may hold values from -6 to 6
- norm_gain: float32 [2048], replicated, may hold values from 0.1 to 1.9
- routes: int32 [1536, 4], P('sp'), may hold values from 0 to 7, all different within a row; in each aligned block of 48 rows (0 to 47, 48 to 95, ...) at most 48 rows name the same one
- route_weight: float32 [1536, 4], P(('sp', 'tp')), may hold values from 0.3 to 1.5
- expert_gate: bfloat16 [8, 2048, 1024], P('sp', None, 'tp'), may hold values from -0.125 to 0.125
- expert_up: bfloat16 [8, 2048, 1024], P('sp', None, 'tp'), may hold values from -0.125 to 0.125
- expert_down: bfloat16 [8, 1024, 2048], P('sp', 'tp'), may hold values from -0.1875 to 0.1875
- shared_gate: bfloat16 [2048, 1024], P(None, 'tp'), may hold values from -0.125 to 0.125
- shared_up: bfloat16 [2048, 1024], P(None, 'tp'), may hold values from -0.125 to 0.125
- shared_down: bfloat16 [1024, 2048], P('tp'), may hold values from -0.1875 to 0.1875
Outputs:
- mixed: bfloat16 [1536, 2048], P(('sp', 'tp'))
Inputs may be any that keep to these rules, and one draw needn't show every extreme that they name: `routes`: the 4 experts of a token are different. In each aligned block of 48 tokens (the tokens of one device after the attention) no expert is named more than 48 times, a bound that some expert reaches in some blocks.
All inputs are finite; a program needn't handle non-finite values.
Results may differ from a plain program's by a relative error of at most 0.018.
Values may be sent and summed in bfloat16 or wider, within the bound.
A program may use at most 128 MiB of HBM per device.

v0:
```python
from functools import partial

import jax
import jax.numpy as jnp
from jax import lax
from jax.sharding import PartitionSpec as P

norm_eps = 1e-06
lowest_score = -1e30


def slot_targets(block_routes, experts, capacity):
    flat_routes = block_routes.reshape(-1)
    onehot = (flat_routes[:, None] == jnp.arange(experts, dtype=jnp.int32)[None, :]).astype(
        jnp.int32
    )
    earlier = jnp.cumsum(onehot, axis=0) - onehot
    return flat_routes * capacity + jnp.sum(earlier * onehot, axis=1)


def build_buffer(token_rows, block_routes, experts, capacity):
    targets = slot_targets(block_routes, experts, capacity)
    row_total = block_routes.shape[0]
    route_count = block_routes.shape[1]
    source_row = jnp.arange(row_total * route_count, dtype=jnp.int32) // route_count
    holder = jnp.full((experts * capacity,), row_total, jnp.int32).at[targets].set(source_row)
    padded = jnp.concatenate(
        [token_rows, jnp.zeros((1, token_rows.shape[1]), token_rows.dtype)], axis=0
    )
    return (padded[holder], targets)


def attention_block(carried, queries, key_block, value_block, score_scale):
    run_max, run_sum, accumulated = carried
    kv_local = run_max.shape[0]
    key_heads = key_block.reshape(key_block.shape[0], kv_local, 2, -1)
    value_heads = value_block.reshape(value_block.shape[0], kv_local, -1)
    scores = (
        jnp.einsum("qagcd,racd->agcqr", queries, key_heads, preferred_element_type=jnp.float32)
        * score_scale
    )
    new_max = jnp.maximum(run_max, jnp.max(scores, axis=-1))
    rescale = jnp.exp(run_max - new_max)
    weights = jnp.exp(scores - new_max[..., None])
    run_sum = run_sum * rescale + jnp.sum(weights, axis=-1)
    update = jnp.einsum(
        "agcqr,rae->agcqe",
        weights.astype(jnp.bfloat16),
        value_heads,
        preferred_element_type=jnp.float32,
    )
    return (new_max, run_sum, accumulated * rescale[..., None] + update)


def fold_keys(carried, pieces, first_row, queries, score_scale):
    key_piece, value_piece = pieces
    total_rows = key_piece.shape[0]
    block_rows = total_rows
    for candidate in (2048, 1024, 512):
        if total_rows % candidate == 0:
            block_rows = candidate
            break
    block_count = total_rows // block_rows

    def block_step(block_index, running):
        start_row = block_index * block_rows
        return attention_block(
            running,
            queries,
            lax.dynamic_slice_in_dim(key_piece, start_row, block_rows, 0),
            lax.dynamic_slice_in_dim(value_piece, start_row, block_rows, 0),
            score_scale,
        )

    return lax.fori_loop(0, block_count, block_step, carried)


def whole_experts(arrived, whole_gate, whole_up, whole_down, senders, capacity, groups):
    local_experts = whole_gate.shape[0]
    width = arrived.shape[-1]
    rows_in = arrived.reshape(senders, local_experts, capacity, width)
    gate_value = jnp.einsum(
        "sjtd,jdf->sjtf", rows_in, whole_gate, preferred_element_type=jnp.float32
    )
    up_value = jnp.einsum("sjtd,jdf->sjtf", rows_in, whole_up, preferred_element_type=jnp.float32)
    hidden = (jax.nn.silu(gate_value) * up_value).astype(jnp.bfloat16)
    hidden_units = hidden.shape[-1]
    hidden = hidden.reshape(senders, local_experts, capacity, groups, hidden_units // groups)
    down_groups = whole_down.reshape(local_experts, groups, hidden_units // groups, width)
    group_sums = jnp.einsum(
        "sjtgf,jgfd->sjtgd", hidden, down_groups, preferred_element_type=jnp.float32
    )
    group_sums = lax.optimization_barrier(group_sums.astype(jnp.bfloat16)).astype(jnp.float32)
    return (
        jnp.sum(group_sums, axis=3)
        .astype(jnp.bfloat16)
        .reshape(senders * local_experts * capacity, width)
    )


def body(
    query_maps,
    key_maps,
    value_rows,
    mix_lambda,
    head_gain,
    out_weight,
    residual,
    norm_gain,
    routes,
    route_weight,
    expert_gate,
    expert_up,
    expert_down,
    shared_gate,
    shared_up,
    shared_down,
):
    local_heads = mix_lambda.shape[0]
    head_width = head_gain.shape[0]
    kv_local = value_rows.shape[1] // head_width
    head_group = local_heads // kv_local
    head_dim = key_maps.shape[1] // (2 * kv_local)
    token_count = query_maps.shape[0]
    queries = query_maps.reshape(token_count, kv_local, head_group, 2, head_dim)
    start_max = jnp.full((kv_local, head_group, 2, token_count), lowest_score, jnp.float32)
    start_sum = jnp.zeros((kv_local, head_group, 2, token_count), jnp.float32)
    start_values = jnp.zeros((kv_local, head_group, 2, token_count, head_width), jnp.float32)
    folder = partial(fold_keys, queries=queries, score_scale=head_dim ** (-0.5))
    run_max, run_sum, accumulated = folder(
        (start_max, start_sum, start_values),
        (
            lax.all_gather(key_maps, "sp", axis=0, tiled=True),
            lax.all_gather(value_rows, "sp", axis=0, tiled=True),
        ),
        jnp.int32(0),
    )
    normalized = accumulated / run_sum[..., None]
    lambdas = mix_lambda.reshape(kv_local, head_group, 1, 1)
    difference = normalized[:, :, 0] - lambdas * normalized[:, :, 1]
    inverse_rms = lax.rsqrt(jnp.mean(difference * difference, axis=-1, keepdims=True) + norm_eps)
    head_scaled = (difference * inverse_rms * head_gain).astype(jnp.bfloat16)
    attended = jnp.transpose(head_scaled, (2, 0, 1, 3)).reshape(
        token_count, local_heads * head_width
    )
    columns = lax.axis_size("tp")
    column = lax.axis_index("tp")
    rows_dev = token_count // columns
    own_rows = lax.dynamic_slice_in_dim(
        out_weight, column * attended.shape[1], attended.shape[1], 0
    )
    projected = lax.psum_scatter(
        jnp.dot(attended, own_rows, preferred_element_type=jnp.float32).astype(jnp.bfloat16),
        "tp",
        scatter_dimension=0,
        tiled=True,
    ).astype(jnp.float32)
    stream = (residual.astype(jnp.float32) + projected).astype(jnp.bfloat16)
    stream_wide = stream.astype(jnp.float32)
    stream_rms = lax.rsqrt(jnp.mean(stream_wide * stream_wide, axis=1, keepdims=True) + norm_eps)
    normed = (stream_wide * stream_rms * norm_gain).astype(jnp.bfloat16)
    senders = lax.axis_size("sp")
    local_experts = expert_gate.shape[0]
    experts = senders * local_experts
    route_count = routes.shape[1]
    capacity = max(2, 2 * rows_dev * route_count // experts)
    local_routed = None
    whole_gate, whole_up, whole_down = (
        lax.all_gather(expert_gate, "tp", axis=2, tiled=True),
        lax.all_gather(expert_up, "tp", axis=2, tiled=True),
        lax.all_gather(expert_down, "tp", axis=1, tiled=True),
    )
    own_routes = lax.dynamic_slice_in_dim(routes, column * rows_dev, rows_dev, 0)
    buffer, targets = build_buffer(normed, own_routes, experts, capacity)
    arrived = lax.all_to_all(buffer, "sp", split_axis=0, concat_axis=0, tiled=True)
    local_routed = whole_experts(
        arrived, whole_gate, whole_up, whole_down, senders, capacity, columns
    )
    shared_rows = lax.all_gather(normed[None], "tp", axis=0, tiled=True)
    shared_in = shared_rows
    shared_in = shared_in.reshape(1 * lax.axis_size("tp") * rows_dev, shared_in.shape[-1])
    shared_hidden = (
        jax.nn.silu(jnp.dot(shared_in, shared_gate, preferred_element_type=jnp.float32))
        * jnp.dot(shared_in, shared_up, preferred_element_type=jnp.float32)
    ).astype(jnp.bfloat16)
    shared_out = jnp.dot(shared_hidden, shared_down, preferred_element_type=jnp.float32)
    pieces = shared_out.reshape(1 * lax.axis_size("tp"), rows_dev, shared_out.shape[-1])
    terms_out = pieces.astype(jnp.bfloat16)
    summed = (
        lax.psum_scatter(
            lax.optimization_barrier(terms_out).astype(jnp.float32).astype(jnp.bfloat16),
            "tp",
            scatter_dimension=0,
            tiled=True,
        )
        .astype(jnp.float32)[0]
        .astype(jnp.bfloat16)
    )
    returned = lax.all_to_all(local_routed, "sp", split_axis=0, concat_axis=0, tiled=True)
    picked = (
        returned[targets].reshape(rows_dev, route_count, returned.shape[-1]).astype(jnp.float32)
    )
    routed_sum = jnp.sum(route_weight[:, :, None] * picked, axis=1)
    return (stream_wide + summed.astype(jnp.float32) + routed_sum).astype(jnp.bfloat16)


def solution(mesh):
    in_specs = (
        P("sp", "tp"),
        P("sp", "tp"),
        P("sp", "tp"),
        P("tp"),
        P(),
        P(),
        P(("sp", "tp"), None),
        P(),
        P("sp", None),
        P(("sp", "tp"), None),
        P("sp", None, "tp"),
        P("sp", None, "tp"),
        P("sp", "tp", None),
        P(None, "tp"),
        P(None, "tp"),
        P("tp", None),
    )
    out_specs = P(("sp", "tp"), None)
    return jax.shard_map(body, mesh=mesh, in_specs=in_specs, out_specs=out_specs, check_vma=False)
```

profile of v0, /device:TPU:0, one launch (start us, length us, event | category | flops | bytes accessed | tf_op | source)
XLA Modules:
  0.0 286.6 jit_solution(18358103989348239714)
XLA Ops:
  6.5 33.1 %all_gather.18 = bf16[1536,128]{1,0:T(8,128)(2,1)S(1)} all-gather(bf16[192,128]{1,0:T(8,128)(2,1)} %param.19), channel_id=1, replica_groups=mesh['sp'=8,'tp'=4] {'sp'}, dimensions={0}, use_global_device_ids=true | all-gather | bytes 442368 | tf_op jit(solution)/shard_map/all_gather | solution.py:133
  39.6 33.3 %all_gather.19 = bf16[1536,128]{1,0:T(8,128)(2,1)} all-gather(bf16[192,128]{1,0:T(8,128)(2,1)} %param.20), channel_id=1, replica_groups=mesh['sp'=8,'tp'=4] {'sp'}, dimensions={0}, use_global_device_ids=true | all-gather | bytes 442368 | tf_op jit(solution)/shard_map/all_gather | solution.py:134
  72.9 1.0 copy.38
  74.0 9.5 %while.18 = (s32[]{:T(128)}, f32[1,2,2,192]{3,1,2,0:T(2,128)S(1)}, f32[1,2,2,192]{3,1,2,0:T(2,128)S(1)}, f32[1,2,2,192,128]{4,3,2,1,0:T(8,128)S(1)}, bf16[1536,1...) while((s32[]{:T(128)}, f32[1,2,2,192]{3,1,2,0:T(2,128)S(1)}, ...), condition=%wide.region_3.0_spmd.clone, body=%wide.region_0.0_spmd.clone.sunk | while | flops 153260544 | bytes 9587943 | solution.py:75
  74.1 0.6 copy-done.1
  74.7 0.5 bitcast_reduce_fusion.2
  75.3 0.4 fusion.66
  75.7 1.3 fusion.67
  77.3 0.6 copy-done.1
  77.9 0.5 bitcast_reduce_fusion.2
  78.4 0.4 fusion.66
  78.9 1.3 fusion.67
  80.5 0.6 copy-done.1
  81.0 0.5 bitcast_reduce_fusion.2
  81.6 0.4 fusion.66
  82.1 1.3 fusion.67
  83.5 0.2 broadcast_divide_fusion
  83.6 0.2 multiply_reduce_fusion.1
  83.9 0.1 fusion.36
  84.1 2.6 convolution_convert_fusion.1
  86.8 0.7 all-gather.5.cloned.1.call-update
  87.5 0.7 all-gather.7.cloned.1.call-update
  88.3 0.5 all-gather.9.cloned.1.call-update
  89.1 0.6 reduce-window.6
  89.7 0.2 slice_reduce_fusion
  90.3 1.2 scatter_custom_fusion
  91.5 19.7 %reduce-scatter.3.cloned.1.call-done = bf16[48,2048]{1,0:T(8,128)(2,1)} async-done(((bf16[192,2048]{1,0:T(8,128)(2,1)}), bf16[48,2048]{1,0:T(8,128)(2,1)}) %reduce-scatter.3.cloned.1.call-update) | async-done | bytes 196624 | tf_op jit(solution)/shard_map/reduce_scatter | solution.py:152
  111.2 1.1 fusion.24
  112.4 1.0 fusion.26
  113.4 0.7 copy-done.6
  114.1 2.5 gather_fusion
  116.6 42.2 %all_to_all.18 = bf16[8,48,2048]{2,1,0:T(8,128)(2,1)} all-to-all(bf16[8,48,2048]{2,1,0:T(8,128)(2,1)S(1)} %bitcast.169), channel_id=1, replica_groups=mesh['sp'=8,'tp'=4] {'sp'}, dimensions={0} | all-to-all | bytes 3145728 | tf_op jit(solution)/shard_map/all_to_all | solution.py:175
  158.8 5.8 %fusion.13 = f32[8,48,1024]{2,1,0:T(8,128)} fusion(bf16[8,48,2048]{2,1,0:T(8,128)(2,1)} %all_to_all.18, bf16[1,2048,1024]{2,1,0:T(8,128)(2,1)} %all-gather.5.cloned.1.call-done), kind=kOutput, calls=%fused_computation.28 | convolution fusion | flops 1610612736 | bytes 7340032 | tf_op jit(solution)/shard_map/sjtd,jdf->sjtf/dot_general | solution.py:82
  164.6 19.8 %all-gather.7.cloned.1.call-done = bf16[1,2048,1024]{2,1,0:T(8,128)(2,1)} async-done(((bf16[1,2048,256]{2,1,0:T(8,128)(2,1)}), bf16[1,2048,1024]{2,1,0:T(8,128)(2,1)}) %all-gather.7.cloned.1.call-update) | async-done | bytes 4194320 | tf_op jit(solution)/shard_map/all_gather | solution.py:170
  184.4 4.6 %fusion.15 = bf16[8,1,48,1024]{3,2,0,1:T(8,128)(2,1)S(1)} fusion(f32[8,48,1024]{2,1,0:T(8,128)} %fusion.13, bf16[8,48,2048]{2,1,0:T(8,128)(2,1)S(1)} %copy-done.7, bf16[1,2048,1024]{2,1,0:T(8,128)(2,1)} %all-gather.7.cloned.1.call-done), kind=kOutput, calls=%fused_computation.33 | convolution fusion | flops 1612972032 | bytes 8126464 | tf_op jit(solution)/shard_map/sjtd,jdf->sjtf/dot_general | solution.py:85
  189.0 0.6 reshape.228
  189.6 30.7 %all-gather.9.cloned.1.call-done = bf16[1,1024,2048]{2,1,0:T(8,128)(2,1)} async-done(((bf16[1,256,2048]{2,1,0:T(8,128)(2,1)}), bf16[1,1024,2048]{2,1,0:T(8,128)(2,1)}) %all-gather.9.cloned.1.call-update) | async-done | bytes 4194320 | tf_op jit(solution)/shard_map/all_gather | solution.py:171
  220.3 6.7 %convert_bitcast_fusion = bf16[8,1,48,4,2048]{4,2,0,3,1:T(8,128)(2,1)} fusion(bf16[4,256,2048,1]{2,1,3,0:T(8,128)(2,1)} %bitcast.170, bf16[8,48,4,256]{3,2,1,0:T(4,128)(2,1)S(1)} %reshape.228), kind=kOutput, calls=%fused_computation.25 | convolution fusion | flops 1613758464 | bytes 11272192 | tf_op jit(solution)/shard_map/sjtgf,jgfd->sjtgd/dot_general | solution.py:90
  227.0 5.7 %reduce_sum.67 = bf16[8,48,2048]{2,1,0:T(8,128)(2,1)} reduce(bf16[8,1,48,4,2048]{4,2,0,3,1:T(8,128)(2,1)} %convert_bitcast_fusion, bf16[]{:T(256)} %constant.104.clone.1), dimensions={1,3}, to_apply=%region_12.13 | reduce | flops 2359296 | bytes 7864322 | tf_op jit(solution)/shard_map/reduce_sum | solution.py:95
  232.6 5.5 %all-to-all-start.1 = ((bf16[8,48,2048]{2,1,0:T(8,128)(2,1)}), bf16[8,48,2048]{2,1,0:T(8,128)(2,1)S(1)}, u32[]{:S(2)}, u32[]{:S(2)}) async-start(bf16[8,48,2048]{2,1,0:T(8,128)(2,1)} %reduce_sum.67), calls=%async_computation.3 | async-start | bytes 3145728 | tf_op jit(solution)/shard_map/all_to_all | solution.py:199
  238.2 8.5 %all-gather = bf16[192,2048]{1,0:T(8,128)(2,1)S(1)} all-gather(bf16[48,2048]{1,0:T(8,128)(2,1)} %copy-done.6), channel_id=2, replica_groups=mesh['sp'=8,'tp'=4] {'tp'}, dimensions={0}, use_global_device_ids=true | all-gather | bytes 983040 | tf_op jit(solution)/shard_map/all_gather | solution.py:179
  246.7 2.3 fusion.46
  249.0 3.2 %convolution_convert_fusion = bf16[192,2048]{1,0:T(8,128)(2,1)} fusion(bf16[256,2048]{1,0:T(8,128)(2,1)S(1)} %copy-done, bf16[192,2048]{1,0:T(8,128)(2,1)S(1)} %all-gather, bf16[2048,256]{1,0:T(8,128)(2,1)} %param.32, f32[192,256]{1,0:T(8,128)} %fusion.46), kind=kOutput, calls=%fused_computation.30 | convolution fusion | flops 403341312 | bytes 3866624 | tf_op jit(solution)/shard_map/dot_general | solution.py:186
  252.3 23.2 %all-to-all-done.1 = bf16[8,48,2048]{2,1,0:T(8,128)(2,1)S(1)} async-done(((bf16[8,48,2048]{2,1,0:T(8,128)(2,1)}), bf16[8,48,2048]{2,1,0:T(8,128)(2,1)S(1)}, u32[]{:S(2)}, u32[]{:S(2)}) %all-to-all-start.1) | async-done | bytes 1572896 | tf_op jit(solution)/shard_map/all_to_all | solution.py:199
  275.5 1.1 gather_fusion.1
  276.7 0.5 reshape.232
  277.2 1.1 multiply_reduce_fusion
  278.4 1.7 fusion.28
  (83 shorter events, 1.7 us)
Async XLA Ops:
  6.5 242.5 %copy-start = (bf16[256,2048]{1,0:T(8,128)(2,1)S(1)}, bf16[256,2048]{1,0:T(8,128)(2,1)}, u32[]{:S(2)}) copy-start(bf16[256,2048]{1,0:T(8,128)(2,1)} %param.33) | copy-start | bytes 3145732
  6.5 104.7 %reduce-scatter.3.cloned.1.call-start = ((), (), s32[]{:S(2)}) async-start(), calls=%async_computation.4 | async-start | bytes 983040 | tf_op jit(solution)/shard_map/reduce_scatter | solution.py:152
  73.9 9.7 %copy-start.10 = (f32[2]{0:T(128)S(1)}, f32[2]{0:T(128)}, u32[]{:S(2)}) copy-start(f32[2]{0:T(128)} %param.21) | copy-start | bytes 28
  74.0 9.9 %copy-start.12 = (f32[128]{0:T(128)S(1)}, f32[128]{0:T(128)}, u32[]{:S(2)}) copy-start(f32[128]{0:T(128)} %param.22) | copy-start | bytes 1540
  74.0 0.7 copy-start.1
  75.7 1.4 copy-start.2
  77.1 0.7 copy-start.1
  78.9 1.4 copy-start.2
  80.3 0.7 copy-start.1
  82.0 1.4 copy-start.2
  86.7 2.1 copy-start.11
  86.7 24.5 %copy-start.3 = (bf16[48,2048]{1,0:T(8,128)(2,1)S(1)}, bf16[48,2048]{1,0:T(8,128)(2,1)}, u32[]{:S(2)}) copy-start(bf16[48,2048]{1,0:T(8,128)(2,1)} %param.24) | copy-start | bytes 589828
  86.7 72.1 %all-gather.5.cloned.1.call-start = ((), (), s32[]{:S(2)}) async-start(), calls=%async_computation.6 | async-start | bytes 5242880 | tf_op jit(solution)/shard_map/all_gather | solution.py:169
  87.5 24.9 %copy-start.8 = (f32[2048]{0:T(1024)S(1)}, f32[2048]{0:T(1024)}, u32[]{:S(2)}) copy-start(f32[2048]{0:T(1024)} %param.25) | copy-start | bytes 24580
  87.5 96.9 %all-gather.7.cloned.1.call-start = ((), (), s32[]{:S(2)}) async-start(), calls=%async_computation.7 | async-start | bytes 5242880 | tf_op jit(solution)/shard_map/all_gather | solution.py:170
  88.2 132.1 %all-gather.9.cloned.1.call-start = ((), (), s32[]{:S(2)}) async-start(), calls=%async_computation.8 | async-start | bytes 5242880 | tf_op jit(solution)/shard_map/all_gather | solution.py:171
  113.4 0.7 copy-start.6
  158.8 25.6 %copy-start.7 = (bf16[8,48,2048]{2,1,0:T(8,128)(2,1)S(1)}, bf16[8,48,2048]{2,1,0:T(8,128)(2,1)}, u32[]{:S(2)}) copy-start(bf16[8,48,2048]{2,1,0:T(8,128)(2,1)} %all_to_all.18) | copy-start | bytes 4718596
  232.6 42.9 %all-to-all-start.1 = ((bf16[8,48,2048]{2,1,0:T(8,128)(2,1)}), bf16[8,48,2048]{2,1,0:T(8,128)(2,1)S(1)}, u32[]{:S(2)}, u32[]{:S(2)}) async-start(bf16[8,48,2048]{2,1,0:T(8,128)(2,1)} %reduce_sum.67), calls=%async_computation.3 | async-start | bytes 3145728 | tf_op jit(solution)/shard_map/all_to_all | solution.py:199
  238.1 40.2 %reduce-scatter.5.cloned.1.call-start = ((), (), s32[]{:S(2)}) async-start(), calls=%async_computation.5 | async-start | bytes 983040 | tf_op jit(solution)/shard_map/reduce_scatter | solution.py:190
  249.0 3.2 %copy-start.9 = (f32[48,4]{0,1:T(4,128)S(1)}, f32[48,4]{0,1:T(4,128)}, u32[]{:S(2)}) copy-start(f32[48,4]{0,1:T(4,128)} %param.27) | copy-start | bytes 2308
  277.2 1.2 copy-start.4
  277.2 1.2 copy-start.5
Sparse Core Ops, SparseCore 0:
  86.8 24.3 reduce-scatter.2
  112.8 34.9 all-gather.4
  149.4 34.9 all-gather.6
  185.8 34.4 all-gather.8
  252.3 23.8 reduce-scatter.4
where the time goes:
time: 287 us
  blocking collectives  117 us (41%)
  waiting for transfers between devices  95.4 us (33%)
  matrix products  30.7 us (11%)
  other arithmetic  13.4 us (5%)
  between operations  13.4 us (5%)
  local copies, waits for them, and re-layouts  10.6 us (4%)
  starting transfers between devices  5.67 us (2%)
    all_to_all x1, blocking collectives, body(): lax.all_to_all(buffer, 'sp', split_axis=0, concat_axis=0, tiled=True)  42.2 us
    all_gather x1, blocking collectives, body(): lax.all_gather(value_rows, 'sp', axis=0, tiled=True)  33.3 us
    all_gather x1, blocking collectives, body(): lax.all_gather(key_maps, 'sp', axis=0, tiled=True)  33.1 us
    all_gather x1, waiting for transfers between devices, body(): lax.all_gather(expert_down, 'tp', axis=1, tiled=True)  30.7 us
    all_to_all x1, waiting for transfers between devices, body(): lax.all_to_all(local_routed, 'sp', split_axis=0, concat_axis=0, tiled=True)  23.2 us
    all_gather x1, waiting for transfers between devices, body(): lax.all_gather(expert_up, 'tp', axis=2, tiled=True)  19.8 us
    reduce_scatter x1, waiting for transfers between devices, body(): lax.psum_scatter(jnp.dot(attended, own_rows, preferred_element_type=jnp.f...  19.7 us
    all_gather x1, blocking collectives, body(): shared_rows = lax.all_gather(normed[None], 'tp', axis=0, tiled=True)  8.53 us
  transfers between devices with their start and end apart: 6, of which 4 were waited for; matrix products, arithmetic and copies ran while one was open for 9% of the time, Pallas kernels for 0%

commit v1 on v0

--- a/solution.py
+++ b/solution.py
@@ -3,6 +3,8 @@
 import jax
 import jax.numpy as jnp
 from jax import lax
+from jax.experimental import pallas as pl
+from jax.experimental.pallas import tpu as pltpu
 from jax.sharding import PartitionSpec as P
 
 norm_eps = 1e-06
@@ -204,6 +206,418 @@
     return (stream_wide + summed.astype(jnp.float32) + routed_sum).astype(jnp.bfloat16)
 
 
+MESH = pl.DeviceIdType.MESH
+
+
+def peer_barrier(peers):
+    barrier = pltpu.get_barrier_semaphore()
+    for peer in peers:
+        pl.semaphore_signal(barrier, inc=1, device_id=peer, device_id_type=MESH)
+    pl.semaphore_wait(barrier, len(peers))
+
+
+def remote(src, dst, send_sem, recv_sem, peer):
+    return pltpu.make_async_remote_copy(
+        src_ref=src,
+        dst_ref=dst,
+        send_sem=send_sem,
+        recv_sem=recv_sem,
+        device_id=peer,
+        device_id_type=MESH,
+    )
+
+
+def grid_place(sp):
+    s = lax.axis_index("sp")
+    t = lax.axis_index("tp")
+    return s, t, s // 2, s % 2, sp // 2
+
+
+def gather_kernel(sp, tp, count, with_tp, *refs):
+    ins, refs = refs[:count], refs[count:]
+    outs, refs = refs[:count], refs[count:]
+    if with_tp:
+        tp_out, refs = refs[0], refs[1:]
+    send_sem, recv_sem, local_sem = refs[:3]
+    s, t, z, x, depth = grid_place(sp)
+    line = [(lax.rem(z + k, depth) * 2 + x, t) for k in range(1, depth)]
+    across = (z * 2 + (1 - x), t)
+    columns = [(s, lax.rem(t + k, tp)) for k in range(1, tp)] if with_tp else []
+    peer_barrier(line + [across] + columns)
+    copies = []
+    arrivals = []
+    for i in range(count):
+        for k in range(depth - 1, 0, -1):
+            copy = remote(
+                ins[i], outs[i].at[s], send_sem.at[i, k], recv_sem.at[i, k], line[k - 1]
+            )
+            copy.start()
+            copies.append(copy)
+            arrivals.append((k, i, copy))
+    for i in range(count):
+        copy = remote(
+            ins[i], outs[i].at[s], send_sem.at[i, depth], recv_sem.at[i, depth], across
+        )
+        copy.start()
+        copies.append(copy)
+    side = []
+    if with_tp:
+        for k in range(1, tp):
+            copy = remote(
+                ins[0],
+                tp_out.at[t],
+                send_sem.at[0, 2 * depth + k],
+                recv_sem.at[0, 2 * depth + k],
+                columns[k - 1],
+            )
+            copy.start()
+            side.append(copy)
+        own = pltpu.make_async_copy(ins[0], tp_out.at[t], local_sem.at[count])
+        own.start()
+    locals_ = []
+    for i in range(count):
+        copy = pltpu.make_async_copy(ins[i], outs[i].at[s], local_sem.at[i])
+        copy.start()
+        locals_.append(copy)
+    order = {1: 0, 3: 1, 2: 2}
+    arrivals.sort(key=lambda item: (order.get(item[0], item[0]), item[1]))
+    for k, i, copy in arrivals:
+        copy.wait_recv()
+        origin = lax.rem(z + depth - k, depth) * 2 + x
+        relay = remote(
+            outs[i].at[origin],
+            outs[i].at[origin],
+            send_sem.at[i, depth + k],
+            recv_sem.at[i, depth + k],
+            across,
+        )
+        relay.start()
+        side.append(relay)
+    for _, _, copy in arrivals:
+        copy.wait_send()
+    for copy in copies:
+        if not any(copy is entry[2] for entry in arrivals):
+            copy.wait()
+    for copy in side:
+        copy.wait()
+    for copy in locals_:
+        copy.wait()
+    if with_tp:
+        own.wait()
+
+
+def gather_sp(arrays, sp, tp, with_tp, collective_id):
+    count = len(arrays)
+    depth = sp // 2
+    shapes = [jax.ShapeDtypeStruct((sp,) + a.shape, a.dtype) for a in arrays]
+    if with_tp:
+        shapes.append(jax.ShapeDtypeStruct((tp,) + arrays[0].shape, arrays[0].dtype))
+    slots = 2 * depth + tp
+    return pl.pallas_call(
+        partial(gather_kernel, sp, tp, count, with_tp),
+        out_shape=tuple(shapes),
+        in_specs=[pl.BlockSpec(memory_space=pltpu.VMEM)] * count,
+        out_specs=tuple([pl.BlockSpec(memory_space=pltpu.VMEM)] * len(shapes)),
+        scratch_shapes=[
+            pltpu.SemaphoreType.DMA((count, slots)),
+            pltpu.SemaphoreType.DMA((count, slots)),
+            pltpu.SemaphoreType.DMA((count + 1,)),
+        ],
+        compiler_params=pltpu.CompilerParams(
+            collective_id=collective_id, has_side_effects=True
+        ),
+        cost_estimate=pl.CostEstimate(flops=0, bytes_accessed=40_000_000, transcendentals=0),
+    )(*arrays)
+
+
+def heads_kernel(tp, x_ref, out_ref, send_sem, recv_sem, local_sem):
+    s = lax.axis_index("sp")
+    t = lax.axis_index("tp")
+    rows = out_ref.shape[0]
+    width = x_ref.shape[1]
+    peers = [(s, lax.rem(t + k, tp)) for k in range(1, tp)]
+    peer_barrier(peers)
+    mine = pl.ds(pl.multiple_of(t * width, width), width)
+    copies = []
+    for k in range(1, tp):
+        target = lax.rem(t + k, tp)
+        copy = remote(
+            x_ref.at[pl.ds(pl.multiple_of(target * rows, rows), rows)],
+            out_ref.at[:, mine],
+            send_sem.at[k],
+            recv_sem.at[k],
+            peers[k - 1],
+        )
+        copy.start()
+        copies.append(copy)
+    own = pltpu.make_async_copy(
+        x_ref.at[pl.ds(pl.multiple_of(t * rows, rows), rows)], out_ref.at[:, mine], local_sem
+    )
+    own.start()
+    for copy in copies:
+        copy.wait()
+    own.wait()
+
+
+def exchange_heads(attended, tp, collective_id):
+    tokens, width = attended.shape
+    return pl.pallas_call(
+        partial(heads_kernel, tp),
+        out_shape=jax.ShapeDtypeStruct((tokens // tp, tp * width), attended.dtype),
+        in_specs=[pl.BlockSpec(memory_space=pltpu.VMEM)],
+        out_specs=pl.BlockSpec(memory_space=pltpu.VMEM),
+        scratch_shapes=[
+            pltpu.SemaphoreType.DMA((tp,)),
+            pltpu.SemaphoreType.DMA((tp,)),
+            pltpu.SemaphoreType.DMA,
+        ],
+        compiler_params=pltpu.CompilerParams(
+            collective_id=collective_id, has_side_effects=True
+        ),
+        cost_estimate=pl.CostEstimate(flops=0, bytes_accessed=10_000_000, transcendentals=0),
+    )(attended)
+
+
+def return_kernel(
+    sp,
+    tp,
+    routed_ref,
+    shared_ref,
+    stream_ref,
+    out_ref,
+    from_across,
+    pair_sum,
+    from_line,
+    from_column,
+    send_sem,
+    recv_sem,
+):
+    s, t, z, x, depth = grid_place(sp)
+    line = [(lax.rem(z + k, depth) * 2 + x, t) for k in range(1, depth)]
+    across = (z * 2 + (1 - x), t)
+    columns = [(s, lax.rem(t + k, tp)) for k in range(1, tp)]
+    peer_barrier(line + [across] + columns)
+    order = [2, 3, 1] if depth == 4 else list(range(1, depth))
+    crossing = {}
+    for k in order + [0]:
+        target = lax.rem(z + k, depth) * 2 + (1 - x)
+        copy = remote(
+            routed_ref.at[target], from_across.at[k], send_sem.at[k], recv_sem.at[k], across
+        )
+        copy.start()
+        crossing[k] = copy
+    side = []
+    for k in range(1, tp):
+        copy = remote(
+            shared_ref.at[lax.rem(t + k, tp)],
+            from_column.at[k - 1],
+            send_sem.at[2 * depth + k],
+            recv_sem.at[2 * depth + k],
+            columns[k - 1],
+        )
+        copy.start()
+        side.append(copy)
+    moving = []
+    for k in order:
+        crossing[k].wait_recv()
+        target = lax.rem(z + k, depth) * 2 + x
+        pair_sum[k - 1] = (
+            routed_ref[target].astype(jnp.float32) + from_across[k].astype(jnp.float32)
+        ).astype(jnp.bfloat16)
+        copy = remote(
+            pair_sum.at[k - 1],
+            from_line.at[k - 1],
+            send_sem.at[depth + k],
+            recv_sem.at[depth + k],
+            line[k - 1],
+        )
+        copy.start()
+        moving.append(copy)
+    total = stream_ref[...].astype(jnp.float32) + shared_ref[t].astype(jnp.float32)
+    for k, copy in enumerate(side):
+        copy.wait_recv()
+        total = total + from_column[k].astype(jnp.float32)
+    crossing[0].wait_recv()
+    total = total + routed_ref[s].astype(jnp.float32) + from_across[0].astype(jnp.float32)
+    for k, copy in zip(order, moving):
+        copy.wait_recv()
+        total = total + from_line[k - 1].astype(jnp.float32)
+    out_ref[...] = total.astype(out_ref.dtype)
+    for copy in list(crossing.values()) + side + moving:
+        copy.wait_send()
+
+
+def return_rows(routed, shared, stream, sp, tp, collective_id):
+    rows, width = stream.shape
+    depth = sp // 2
+    slots = 2 * depth + tp
+    return pl.pallas_call(
+        partial(return_kernel, sp, tp),
+        out_shape=jax.ShapeDtypeStruct((rows, width), jnp.bfloat16),
+        in_specs=[pl.BlockSpec(memory_space=pltpu.VMEM)] * 3,
+        out_specs=pl.BlockSpec(memory_space=pltpu.VMEM),
+        scratch_shapes=[
+            pltpu.VMEM((depth, rows, width), jnp.bfloat16),
+            pltpu.VMEM((depth - 1, rows, width), jnp.bfloat16),
+            pltpu.VMEM((depth - 1, rows, width), jnp.bfloat16),
+            pltpu.VMEM((tp - 1, rows, width), jnp.bfloat16),
+            pltpu.SemaphoreType.DMA((slots,)),
+            pltpu.SemaphoreType.DMA((slots,)),
+        ],
+        compiler_params=pltpu.CompilerParams(
+            collective_id=collective_id, has_side_effects=True
+        ),
+        cost_estimate=pl.CostEstimate(flops=0, bytes_accessed=60_000_000, transcendentals=0),
+    )(routed, shared, stream)
+
+
+def experts_kernel(groups, *refs):
+    rows_ref, weight_ref = refs[:2]
+    triples = [refs[2 + 3 * q : 5 + 3 * q] for q in range(groups)]
+    out_ref, gate_buf, up_buf, down_buf, total, sems = refs[2 + 3 * groups :]
+    copies = []
+    for q in range(groups):
+        for n, (source, buffer) in enumerate(zip(triples[q], (gate_buf, up_buf, down_buf))):
+            copy = pltpu.make_async_copy(source, buffer.at[q], sems.at[q, n])
+            copy.start()
+            copies.append(copy)
+    for q in range(groups):
+        copies[3 * q].wait()
+        gate_value = jnp.dot(rows_ref[...], gate_buf[q], preferred_element_type=jnp.float32)
+        copies[3 * q + 1].wait()
+        up_value = jnp.dot(rows_ref[...], up_buf[q], preferred_element_type=jnp.float32)
+        hidden = (jax.nn.silu(gate_value) * up_value).astype(jnp.bfloat16)
+        copies[3 * q + 2].wait()
+        product = jnp.dot(hidden, down_buf[q], preferred_element_type=jnp.float32)
+        if q == 0:
+            total[...] = product
+        elif q < groups - 1:
+            total[...] += product
+        else:
+            out_ref[...] = ((total[...] + product) * weight_ref[...]).astype(jnp.bfloat16)
+
+
+def run_experts(rows_in, dense_weight, triples):
+    groups = len(triples)
+    count, width = rows_in.shape
+    units = triples[0][0].shape[1]
+    flat = [array for triple in triples for array in triple]
+    return pl.pallas_call(
+        partial(experts_kernel, groups),
+        out_shape=jax.ShapeDtypeStruct((count, width), jnp.bfloat16),
+        in_specs=[pl.BlockSpec(memory_space=pltpu.VMEM)] * 2
+        + [pl.BlockSpec(memory_space=pl.ANY)] * len(flat),
+        out_specs=pl.BlockSpec(memory_space=pltpu.VMEM),
+        scratch_shapes=[
+            pltpu.VMEM((groups, width, units), jnp.bfloat16),
+            pltpu.VMEM((groups, width, units), jnp.bfloat16),
+            pltpu.VMEM((groups, units, width), jnp.bfloat16),
+            pltpu.VMEM((count, width), jnp.float32),
+            pltpu.SemaphoreType.DMA((groups, 3)),
+        ],
+        compiler_params=pltpu.CompilerParams(vmem_limit_bytes=40 * 1024 * 1024),
+        cost_estimate=pl.CostEstimate(
+            flops=6 * count * width * units * groups,
+            bytes_accessed=12_000_000,
+            transcendentals=0,
+        ),
+    )(rows_in, dense_weight, *flat)
+
+
+def dense_body(
+    query_maps,
+    key_maps,
+    value_rows,
+    mix_lambda,
+    head_gain,
+    out_weight,
+    residual,
+    norm_gain,
+    routes,
+    route_weight,
+    expert_gate,
+    expert_up,
+    expert_down,
+    shared_gate,
+    shared_up,
+    shared_down,
+):
+    sp = lax.axis_size("sp")
+    tp = lax.axis_size("tp")
+    s = lax.axis_index("sp")
+    t = lax.axis_index("tp")
+
+    def swapped(array, step):
+        return lax.ppermute(array, "tp", [(i, i ^ step) for i in range(tp)])
+
+    own = (expert_gate[0], expert_up[0], expert_down[0])
+    far = tuple(swapped(a, 2) for a in own)
+    near = tuple(swapped(a, 1) for a in own)
+    near_far = tuple(swapped(a, 1) for a in far)
+
+    local_heads = mix_lambda.shape[0]
+    head_width = head_gain.shape[0]
+    kv_local = value_rows.shape[1] // head_width
+    head_group = local_heads // kv_local
+    head_dim = key_maps.shape[1] // (2 * kv_local)
+    token_count = query_maps.shape[0]
+    rows_dev = token_count // tp
+    experts = sp
+
+    own_routes = lax.dynamic_slice_in_dim(routes, t * rows_dev, rows_dev, 0)
+    named = own_routes[None, :, :] == jnp.arange(experts, dtype=jnp.int32)[:, None, None]
+    table = jnp.sum(jnp.where(named, route_weight[None], 0.0), axis=2)
+    lanes = -(-rows_dev // 128) * 128
+    table = jnp.pad(table, ((0, 0), (0, lanes - rows_dev)))
+
+    key_all, value_all, tables = gather_sp([key_maps, value_rows, table], sp, tp, False, 1)
+    key_all = key_all.reshape(sp * token_count, -1)
+    value_all = value_all.reshape(sp * token_count, -1)
+    dense_weight = lax.dynamic_index_in_dim(tables, s, 1, False)[:, :rows_dev]
+    dense_weight = dense_weight.reshape(sp * rows_dev, 1)
+
+    queries = query_maps.reshape(token_count, kv_local, head_group, 2, head_dim)
+    start_max = jnp.full((kv_local, head_group, 2, token_count), lowest_score, jnp.float32)
+    start_sum = jnp.zeros((kv_local, head_group, 2, token_count), jnp.float32)
+    start_values = jnp.zeros((kv_local, head_group, 2, token_count, head_width), jnp.float32)
+    run_max, run_sum, accumulated = fold_keys(
+        (start_max, start_sum, start_values),
+        (key_all, value_all),
+        jnp.int32(0),
+        queries,
+        head_dim ** (-0.5),
+    )
+    normalized = accumulated / run_sum[..., None]
+    lambdas = mix_lambda.reshape(kv_local, head_group, 1, 1)
+    difference = normalized[:, :, 0] - lambdas * normalized[:, :, 1]
+    inverse_rms = lax.rsqrt(jnp.mean(difference * difference, axis=-1, keepdims=True) + norm_eps)
+    head_scaled = (difference * inverse_rms * head_gain).astype(jnp.bfloat16)
+    attended = jnp.transpose(head_scaled, (2, 0, 1, 3)).reshape(
+        token_count, local_heads * head_width
+    )
+    attended = exchange_heads(attended, tp, 2)
+    projected = jnp.dot(attended, out_weight, preferred_element_type=jnp.float32)
+    stream = (residual.astype(jnp.float32) + projected).astype(jnp.bfloat16)
+    stream_wide = stream.astype(jnp.float32)
+    stream_rms = lax.rsqrt(jnp.mean(stream_wide * stream_wide, axis=1, keepdims=True) + norm_eps)
+    normed = (stream_wide * stream_rms * norm_gain).astype(jnp.bfloat16)
+
+    routed_in, shared_in = gather_sp([normed], sp, tp, True, 3)
+    width = normed.shape[1]
+    shared_in = shared_in.reshape(tp * rows_dev, width)
+    shared_hidden = (
+        jax.nn.silu(jnp.dot(shared_in, shared_gate, preferred_element_type=jnp.float32))
+        * jnp.dot(shared_in, shared_up, preferred_element_type=jnp.float32)
+    ).astype(jnp.bfloat16)
+    shared_out = jnp.dot(shared_hidden, shared_down, preferred_element_type=jnp.float32)
+    shared_out = shared_out.astype(jnp.bfloat16).reshape(tp, rows_dev, width)
+
+    routed = run_experts(
+        routed_in.reshape(sp * rows_dev, width), dense_weight, (own, near, far, near_far)
+    )
+    return return_rows(routed.reshape(sp, rows_dev, width), shared_out, stream, sp, tp, 4)
+
+
 def solution(mesh):
     in_specs = (
         P("sp", "tp"),
@@ -224,4 +638,16 @@
         P("tp", None),
     )
     out_specs = P(("sp", "tp"), None)
-    return jax.shard_map(body, mesh=mesh, in_specs=in_specs, out_specs=out_specs, check_vma=False)
+    sp, tp = mesh.shape["sp"], mesh.shape["tp"]
+
+    def chosen(*args):
+        route_count = args[8].shape[1]
+        experts = sp * args[10].shape[0]
+        rows_dev = args[6].shape[0]
+        whole_blocks = 2 * rows_dev * route_count >= experts * rows_dev
+        dense = whole_blocks and args[10].shape[0] == 1 and sp == 8 and tp == 4
+        return (dense_body if dense else body)(*args)
+
+    return jax.shard_map(
+        chosen, mesh=mesh, in_specs=in_specs, out_specs=out_specs, check_vma=False
+    )

time: 287 us -> 165 us (0.57)
  Pallas kernels: 0 us -> 131 us
  blocking collectives: 117 us -> 0 us
  waiting for transfers between devices: 95.4 us -> 0.02 us
  matrix products: 30.7 us -> 11.7 us
  between operations: 13.4 us -> 0.26 us
  other arithmetic: 13.4 us -> 3.44 us
    pallas_call x0 -> x5, Pallas kernels: none -> 131 us  [the longest x2 56.3 us: gather_sp(): pl.pallas_call(partial(gather_kernel, sp, tp, count, with_tp), out_shape=...]
    all_gather x3 -> x0, blocking collectives: 74.9 us -> none  [the longest x1 33.3 us: body(): lax.all_gather(value_rows, 'sp', axis=0, tiled=True)]
    all_gather x3 -> x0, waiting for transfers between devices: 50.5 us -> none  [the longest x1 30.7 us: body(): lax.all_gather(expert_down, 'tp', axis=1, tiled=True)]
    all_to_all x1 -> x0, blocking collectives: 42.2 us -> none  [body(): lax.all_to_all(buffer, 'sp', split_axis=0, concat_axis=0, tiled=True)]
    all_to_all x1 -> x0, waiting for transfers between devices: 23.2 us -> none  [body(): lax.all_to_all(local_routed, 'sp', split_axis=0, concat_axis=0, tiled=True)]
    reduce_scatter x2 -> x0, waiting for transfers between devices: 19.7 us -> none  [the longest x1 19.7 us: body(): lax.psum_scatter(jnp.dot(attended, own_rows, preferred_element_type=jnp.f...]
    dot_general x6 -> x3, matrix products: 25.1 us -> 8.98 us  [the longest x1 3.53 us: dense_body(): jnp.dot(shared_hidden, shared_down, preferred_element_type=jnp.float32)]
    reduce_sum x5 -> x2, other arithmetic: 8.11 us -> 0.9 us  [the longest x1 0.69 us: dense_body(): table = jnp.sum(jnp.where(named, route_weight[None], 0.0), axis=2)]
  transfers between devices with their start and end apart: 6 -> 9, of which waited for: 4 -> 0; matrix products, arithmetic and copies ran while one was open for 9% -> 14% of each run, Pallas kernels for 0% -> 56%
where the time goes in v1:
time: 165 us
  Pallas kernels  131 us (79%)
  local copies, waits for them, and re-layouts  12.1 us (7%)
  matrix products  11.7 us (7%)
  starting transfers between devices  6.34 us (4%)
  other arithmetic  3.44 us (2%)
    pallas_call x2, Pallas kernels, gather_sp(): pl.pallas_call(partial(gather_kernel, sp, tp, count, with_tp), out_shape=...  56.3 us
    pallas_call x1, Pallas kernels, exchange_heads(): pl.pallas_call(partial(heads_kernel, tp), out_shape=jax.ShapeDtypeStruct(...  35.5 us
    pallas_call x1, Pallas kernels, return_rows(): pl.pallas_call(partial(return_kernel, sp, tp), out_shape=jax.ShapeDtypeSt...  27.1 us
    pallas_call x1, Pallas kernels, run_experts(): pl.pallas_call(partial(experts_kernel, groups), out_shape=jax.ShapeDtypeS...  11.7 us
    unnamed x26, local copies, waits for them, and re-layouts  6.67 us
    ppermute x9, starting transfers between devices, swapped(): return lax.ppermute(array, 'tp', [(i, i ^ step) for i in range(tp)])  6.34 us
    dot_general x1, matrix products, dense_body(): jnp.dot(shared_hidden, shared_down, preferred_element_type=jnp.float32)  3.53 us
  transfers between devices with their start and end apart: 9, of which 0 were waited for; matrix products, arithmetic and copies ran while one was open for 14% of the time, Pallas kernels for 56%

profile of v1, /device:TPU:0, one launch (start us, length us, event | category | flops | bytes accessed | tf_op | source)
XLA Modules:
  0.0 164.7 jit_solution(9717738481462599065)
XLA Ops:
  0.0 3.0 %collective-permute-start.3 = (bf16[2048,256]{1,0:T(8,128)(2,1)}, bf16[2048,256]{1,0:T(8,128)(2,1)}, u32[]{:S(2)}, u32[]{:S(2)}) collective-permute-start(bf16[2048,256]{1,0:T(8,128)(2,1)} %bitcast.114), channel_id=1, source_target_pairs={{0,2},{1,3},{2,0},{3,1},{4,6},{5,7},{6,4},{7,5},{8,10},{9,11},{10,... | collective-permute-start | bytes 3145736 | tf_op jit(solution)/shard_map/ppermute | solution.py:551
  3.0 0.1 collective-permute-start.4
  3.1 0.4 collective-permute-start.1
  3.5 1.7 %collective-permute-start.5 = (bf16[256,2048]{1,0:T(8,128)(2,1)}, bf16[256,2048]{1,0:T(8,128)(2,1)}, u32[]{:S(2)}, u32[]{:S(2)}) collective-permute-start(bf16[256,2048]{1,0:T(8,128)(2,1)} %bitcast.11.refs_4_), channel_id=1, source_target_pairs={{0,2},{1,3},{2,0},{3,1},{4,6},{5,7},{6,4},{7,5},{8,10},{9,11},{10,... | collective-permute-start | bytes 3145736 | tf_op jit(solution)/shard_map/ppermute | solution.py:551
  5.3 1.0 copy.38
  6.3 0.8 constant_dynamic-slice_fusion.2
  7.0 0.7 select_reduce_fusion
  7.7 0.6 pad.4.refs_2_
  8.3 20.2 %shard_map.154 = (bf16[8,192,128]{2,1,0:T(8,128)(2,1)}, bf16[8,192,128]{2,1,0:T(8,128)(2,1)S(1)}, f32[8,8,128]{2,1,0:T(8,128)}) custom-call(bf16[192,128]{1,0:T(8,128)(2,1)} %refs_0_.1, bf16[192,128]{1,0:T(8,128)(2,1)} %refs_1_.1, f32[8,128]{1,0:T(8,128)} %pad.4.refs_2_), custom_call_target="tpu_custom_call" | custom-call | bytes 40000000 | tf_op jit(solution)/shard_map/pallas_call | solution.py:316
  28.5 7.5 %while.18 = (s32[]{:T(128)}, f32[1,2,2,192]{3,1,2,0:T(2,128)S(1)}, f32[1,2,2,192]{3,1,2,0:T(2,128)S(1)}, f32[1,2,2,192,128]{4,3,2,1,0:T(8,128)S(1)}, bf16[1536,1...) while((s32[]{:T(128)}, f32[1,2,2,192]{3,1,2,0:T(2,128)S(1)}, ...), condition=%wide.region_4.5_spmd.clone, body=%wide.region_1.4_spmd.clone.sunk | while | flops 153260544 | bytes 6443191 | solution.py:77
  28.6 0.9 constant_dynamic-slice_fusion.4
  29.5 0.1 copy.58
  29.6 0.5 bitcast_reduce_fusion.2
  30.2 0.4 fusion.45
  30.6 0.4 fusion.46
  31.1 0.9 constant_dynamic-slice_fusion.4
  32.0 0.1 copy.58
  32.1 0.5 bitcast_reduce_fusion.2
  32.7 0.4 fusion.45
  33.1 0.4 fusion.46
  33.6 0.9 constant_dynamic-slice_fusion.4
  34.5 0.1 copy.58
  34.6 0.5 bitcast_reduce_fusion.2
  35.2 0.4 fusion.45
  35.6 0.4 fusion.46
  36.0 0.2 broadcast_divide_fusion
  36.2 0.2 multiply_reduce_fusion
  36.5 0.1 fusion.23
  36.6 0.1 copy.43
  36.7 0.7 copy.53
  37.4 35.5 %shard_map.155 = bf16[48,1024]{1,0:T(8,128)(2,1)} custom-call(bf16[192,256]{1,0:T(8,128)(2,1)} %bitcast.129), custom_call_target="tpu_custom_call" | custom-call | bytes 10000000 | tf_op jit(solution)/shard_map/pallas_call | solution.py:364
  72.8 0.8 constant_dynamic-slice_fusion.1
  73.6 0.1 reshape.171.refs_1_
  73.7 3.3 %fusion.13 = (f32[48]{0:T(128)S(1)}, bf16[48,2048]{1,0:T(8,128)(2,1)S(1)}) fusion(bf16[48,1024]{1,0:T(8,128)(2,1)} %shard_map.155, bf16[1024,2048]{1,0:T(8,128)(2,1)} %param.23, bf16[48,2048]{1,0:T(8,128)(2,1)} %param.24), kind=kOutput, calls=%fused_computation.29 | convolution fusion | flops 201916368 | bytes 4686016 | tf_op jit(solution)/shard_map/dot_general | solution.py:599
  77.0 0.2 collective-permute-start.2
  77.2 1.0 copy-done.4
  78.2 0.4 collective-permute-start.6
  78.6 0.1 collective-permute-start.7
  78.7 0.4 collective-permute-start.8
  79.1 0.8 fusion.15.refs_0_
  79.9 36.1 %shard_map.156 = (bf16[8,48,2048]{2,1,0:T(8,128)(2,1)}, bf16[4,48,2048]{2,1,0:T(8,128)(2,1)}) custom-call(bf16[48,2048]{1,0:T(8,128)(2,1)} %fusion.15.refs_0_), custom_call_target="tpu_custom_call" | custom-call | bytes 40000000 | tf_op jit(solution)/shard_map/pallas_call | solution.py:316
  116.1 2.2 %fusion.26 = f32[192,256]{1,0:T(8,128)} fusion(bf16[192,2048]{1,0:T(8,128)(2,1)} %bitcast.122, bf16[2048,256]{1,0:T(8,128)(2,1)S(1)} %copy-done.7), kind=kOutput, calls=%fused_computation.54 | convolution fusion | flops 201326592 | bytes 2031616 | tf_op jit(solution)/shard_map/dot_general | solution.py:609
  118.2 3.5 %convolution_convert_fusion = bf16[192,2048]{1,0:T(8,128)(2,1)} fusion(bf16[256,2048]{1,0:T(8,128)(2,1)S(1)} %copy-done, bf16[192,2048]{1,0:T(8,128)(2,1)} %bitcast.123, bf16[2048,256]{1,0:T(8,128)(2,1)} %param.32, f32[192,256]{1,0:T(8,128)} %fusion.26), kind=kOutput, calls=%fused_computation.22 | convolution fusion | flops 403341312 | bytes 3866624 | tf_op jit(solution)/shard_map/dot_general | solution.py:612
  121.8 1.2 copy-done.5
  123.1 11.7 %shard_map.157 = bf16[384,2048]{1,0:T(8,128)(2,1)S(1)} custom-call(bf16[384,2048]{1,0:T(8,128)(2,1)} %bitcast.132, f32[384,1]{1,0:T(8,128)S(1)} %reshape.171.refs_1_, bf16[2048,256]{1,0:T(8,128)(2,1)S(1)} %bitcast.116, bf16[2048,256]{1,0:T(8,128)(2,1)S(1)} %bitcast.119, bf16[256,2048]{1,0:T(8,128)(2,1)} %bitcast.11.refs_4_, bf16[2048,256]{1,0:T(8,128)(2,1)S(1)} %copy-done.5, ...), custom_call_target="tpu_custom_call" | custom-call | flops 4831838208 | bytes 12000000 | tf_op jit(solution)/shard_map/pallas_call | solution.py:505
  134.8 1.2 copy-done.1
  135.9 27.1 %shard_map.158 = bf16[48,2048]{1,0:T(8,128)(2,1)} custom-call(bf16[8,48,2048]{2,1,0:T(8,128)(2,1)} %bitcast.113, bf16[4,48,2048]{2,1,0:T(8,128)(2,1)} %bitcast.121, bf16[48,2048]{1,0:T(8,128)(2,1)} %copy-done.6), custom_call_target="tpu_custom_call" | custom-call | bytes 60000000 | tf_op jit(solution)/shard_map/pallas_call | solution.py:454
  163.0 1.6 copy.73
  (48 shorter events, 0.2 us)
Async XLA Ops:
  0.0 118.2 %copy-start = (bf16[256,2048]{1,0:T(8,128)(2,1)S(1)}, bf16[256,2048]{1,0:T(8,128)(2,1)}, u32[]{:S(2)}) copy-start(bf16[256,2048]{1,0:T(8,128)(2,1)} %param.33) | copy-start | bytes 3145732
  0.0 77.0 %collective-permute-start.3 = (bf16[2048,256]{1,0:T(8,128)(2,1)}, bf16[2048,256]{1,0:T(8,128)(2,1)}, u32[]{:S(2)}, u32[]{:S(2)}) collective-permute-start(bf16[2048,256]{1,0:T(8,128)(2,1)} %bitcast.114), channel_id=1, source_target_pairs={{0,2},{1,3},{2,0},{3,1},{4,6},{5,7},{6,4},{7,5},{8,10},{9,11},{10,... | collective-permute-start | bytes 3145736 | tf_op jit(solution)/shard_map/ppermute | solution.py:551
  3.0 74.2 %collective-permute-start = (bf16[2048,256]{1,0:T(8,128)(2,1)}, bf16[2048,256]{1,0:T(8,128)(2,1)S(1)}, u32[]{:S(2)}, u32[]{:S(2)}) collective-permute-start(bf16[2048,256]{1,0:T(8,128)(2,1)} %bitcast.115), channel_id=1, source_target_pairs={{0,1},{1,0},{2,3},{3,2},{4,5},{5,4},{6,7},{7,6},{8,9},{9,8},{10,11... | collective-permute-start | bytes 3145736 | tf_op jit(solution)/shard_map/ppermute | solution.py:551
  3.0 75.6 %collective-permute-start.4 = (bf16[2048,256]{1,0:T(8,128)(2,1)}, bf16[2048,256]{1,0:T(8,128)(2,1)}, u32[]{:S(2)}, u32[]{:S(2)}) collective-permute-start(bf16[2048,256]{1,0:T(8,128)(2,1)} %bitcast.117), channel_id=1, source_target_pairs={{0,2},{1,3},{2,0},{3,1},{4,6},{5,7},{6,4},{7,5},{8,10},{9,11},{10,... | collective-permute-start | bytes 3145736 | tf_op jit(solution)/shard_map/ppermute | solution.py:551
  3.1 118.6 %collective-permute-start.1 = (bf16[2048,256]{1,0:T(8,128)(2,1)}, bf16[2048,256]{1,0:T(8,128)(2,1)}, u32[]{:S(2)}, u32[]{:S(2)}) collective-permute-start(bf16[2048,256]{1,0:T(8,128)(2,1)} %bitcast.118), channel_id=1, source_target_pairs={{0,1},{1,0},{2,3},{3,2},{4,5},{5,4},{6,7},{7,6},{8,9},{9,8},{10,11... | collective-permute-start | bytes 3145736 | tf_op jit(solution)/shard_map/ppermute | solution.py:551
  3.5 75.2 %collective-permute-start.5 = (bf16[256,2048]{1,0:T(8,128)(2,1)}, bf16[256,2048]{1,0:T(8,128)(2,1)}, u32[]{:S(2)}, u32[]{:S(2)}) collective-permute-start(bf16[256,2048]{1,0:T(8,128)(2,1)} %bitcast.11.refs_4_), channel_id=1, source_target_pairs={{0,2},{1,3},{2,0},{3,1},{4,6},{5,7},{6,4},{7,5},{8,10},{9,11},{10,... | collective-permute-start | bytes 3145736 | tf_op jit(solution)/shard_map/ppermute | solution.py:551
  28.5 7.7 %copy-start.9 = (f32[2]{0:T(128)S(1)}, f32[2]{0:T(128)}, u32[]{:S(2)}) copy-start(f32[2]{0:T(128)} %param.21) | copy-start | bytes 28
  28.5 7.9 %copy-start.10 = (f32[128]{0:T(128)S(1)}, f32[128]{0:T(128)}, u32[]{:S(2)}) copy-start(f32[128]{0:T(128)} %param.22) | copy-start | bytes 1540
  73.7 5.4 %copy-start.8 = (f32[2048]{0:T(1024)S(1)}, f32[2048]{0:T(1024)}, u32[]{:S(2)}) copy-start(f32[2048]{0:T(1024)} %param.25) | copy-start | bytes 24580
  73.7 42.3 %copy-start.7 = (bf16[2048,256]{1,0:T(8,128)(2,1)S(1)}, bf16[2048,256]{1,0:T(8,128)(2,1)}, u32[]{:S(2)}) copy-start(bf16[2048,256]{1,0:T(8,128)(2,1)} %param.31) | copy-start | bytes 3145732
  77.0 57.7 %copy-start.6 = (bf16[48,2048]{1,0:T(8,128)(2,1)}, bf16[48,2048]{1,0:T(8,128)(2,1)S(1)}, u32[]{:S(2)}) copy-start(bf16[48,2048]{1,0:T(8,128)(2,1)S(1)} %get-tuple-element.208.stream_ref) | copy-start | bytes 589828
  77.0 44.7 %collective-permute-start.2 = (bf16[256,2048]{1,0:T(8,128)(2,1)}, bf16[256,2048]{1,0:T(8,128)(2,1)}, u32[]{:S(2)}, u32[]{:S(2)}) collective-permute-start(bf16[256,2048]{1,0:T(8,128)(2,1)} %bitcast.11.refs_4_), channel_id=1, source_target_pairs={{0,1},{1,0},{2,3},{3,2},{4,5},{5,4},{6,7},{7,6},{8,9},{9,8},{10,11... | collective-permute-start | bytes 3145736 | tf_op jit(solution)/shard_map/ppermute | solution.py:551
  77.2 1.0 copy-start.4
  78.2 43.6 %collective-permute-start.6 = (bf16[2048,256]{1,0:T(8,128)(2,1)}, bf16[2048,256]{1,0:T(8,128)(2,1)}, u32[]{:S(2)}, u32[]{:S(2)}) collective-permute-start(bf16[2048,256]{1,0:T(8,128)(2,1)} %collective-permute-done.3.refs_8_), channel_id=1, source_target_pairs={{0,1},{1,0},{2,3},{3,2},{4,5},{5,4},{6,7},{7,6},{8,9},{9,8},{10,11... | collective-permute-start | bytes 3145736 | tf_op jit(solution)/shard_map/ppermute | solution.py:551
  78.6 43.2 %collective-permute-start.7 = (bf16[2048,256]{1,0:T(8,128)(2,1)}, bf16[2048,256]{1,0:T(8,128)(2,1)}, u32[]{:S(2)}, u32[]{:S(2)}) collective-permute-start(bf16[2048,256]{1,0:T(8,128)(2,1)} %collective-permute-done.4.refs_9_), channel_id=1, source_target_pairs={{0,1},{1,0},{2,3},{3,2},{4,5},{5,4},{6,7},{7,6},{8,9},{9,8},{10,11... | collective-permute-start | bytes 3145736 | tf_op jit(solution)/shard_map/ppermute | solution.py:551
  78.7 43.1 %collective-permute-start.8 = (bf16[256,2048]{1,0:T(8,128)(2,1)}, bf16[256,2048]{1,0:T(8,128)(2,1)}, u32[]{:S(2)}, u32[]{:S(2)}) collective-permute-start(bf16[256,2048]{1,0:T(8,128)(2,1)} %collective-permute-done.5.refs_10_), channel_id=1, source_target_pairs={{0,1},{1,0},{2,3},{3,2},{4,5},{5,4},{6,7},{7,6},{8,9},{9,8},{10,11... | collective-permute-start | bytes 3145736 | tf_op jit(solution)/shard_map/ppermute | solution.py:551
  118.2 3.6 %copy-start.2 = (bf16[1,2048,256]{2,1,0:T(8,128)(2,1)S(1)}, bf16[1,2048,256]{2,1,0:T(8,128)(2,1)}, u32[]{:S(2)}) copy-start(bf16[1,2048,256]{2,1,0:T(8,128)(2,1)} %param.28) | copy-start | bytes 3145732
  118.2 3.6 %copy-start.3 = (bf16[1,2048,256]{2,1,0:T(8,128)(2,1)S(1)}, bf16[1,2048,256]{2,1,0:T(8,128)(2,1)}, u32[]{:S(2)}) copy-start(bf16[1,2048,256]{2,1,0:T(8,128)(2,1)} %param.29) | copy-start | bytes 3145732
  121.8 1.2 copy-start.5
  134.8 1.2 copy-start.1

commit v2 on v1

--- a/solution.py
+++ b/solution.py
@@ -6,6 +6,7 @@
 from jax.experimental import pallas as pl
 from jax.experimental.pallas import tpu as pltpu
 from jax.sharding import PartitionSpec as P
+
 
 norm_eps = 1e-06
 lowest_score = -1e30
@@ -129,7 +130,7 @@
     start_sum = jnp.zeros((kv_local, head_group, 2, token_count), jnp.float32)
     start_values = jnp.zeros((kv_local, head_group, 2, token_count, head_width), jnp.float32)
     folder = partial(fold_keys, queries=queries, score_scale=head_dim ** (-0.5))
-    run_max, run_sum, accumulated = folder(
+    _, run_sum, accumulated = folder(
         (start_max, start_sum, start_values),
         (
             lax.all_gather(key_maps, "sp", axis=0, tiled=True),
@@ -333,37 +334,29 @@
 def heads_kernel(tp, x_ref, out_ref, send_sem, recv_sem, local_sem):
     s = lax.axis_index("sp")
     t = lax.axis_index("tp")
-    rows = out_ref.shape[0]
     width = x_ref.shape[1]
     peers = [(s, lax.rem(t + k, tp)) for k in range(1, tp)]
     peer_barrier(peers)
     mine = pl.ds(pl.multiple_of(t * width, width), width)
     copies = []
     for k in range(1, tp):
-        target = lax.rem(t + k, tp)
         copy = remote(
-            x_ref.at[pl.ds(pl.multiple_of(target * rows, rows), rows)],
-            out_ref.at[:, mine],
-            send_sem.at[k],
-            recv_sem.at[k],
-            peers[k - 1],
+            x_ref, out_ref.at[:, mine], send_sem.at[k], recv_sem.at[k], peers[k - 1]
         )
         copy.start()
         copies.append(copy)
-    own = pltpu.make_async_copy(
-        x_ref.at[pl.ds(pl.multiple_of(t * rows, rows), rows)], out_ref.at[:, mine], local_sem
-    )
+    own = pltpu.make_async_copy(x_ref, out_ref.at[:, mine], local_sem)
     own.start()
     for copy in copies:
         copy.wait()
     own.wait()
 
 
-def exchange_heads(attended, tp, collective_id):
+def gather_heads(attended, tp, collective_id):
     tokens, width = attended.shape
     return pl.pallas_call(
         partial(heads_kernel, tp),
-        out_shape=jax.ShapeDtypeStruct((tokens // tp, tp * width), attended.dtype),
+        out_shape=jax.ShapeDtypeStruct((tokens, tp * width), attended.dtype),
         in_specs=[pl.BlockSpec(memory_space=pltpu.VMEM)],
         out_specs=pl.BlockSpec(memory_space=pltpu.VMEM),
         scratch_shapes=[
@@ -374,7 +367,7 @@
         compiler_params=pltpu.CompilerParams(
             collective_id=collective_id, has_side_effects=True
         ),
-        cost_estimate=pl.CostEstimate(flops=0, bytes_accessed=10_000_000, transcendentals=0),
+        cost_estimate=pl.CostEstimate(flops=0, bytes_accessed=20_000_000, transcendentals=0),
     )(attended)
 
 
@@ -473,21 +466,29 @@
 
 def experts_kernel(groups, *refs):
     rows_ref, weight_ref = refs[:2]
-    triples = [refs[2 + 3 * q : 5 + 3 * q] for q in range(groups)]
-    out_ref, gate_buf, up_buf, down_buf, total, sems = refs[2 + 3 * groups :]
+    parts = [refs[2 + 4 * q : 6 + 4 * q] for q in range(groups)]
+    out_ref, gate_buf, up_buf, down_buf, total, sems = refs[2 + 4 * groups :]
     copies = []
     for q in range(groups):
-        for n, (source, buffer) in enumerate(zip(triples[q], (gate_buf, up_buf, down_buf))):
-            copy = pltpu.make_async_copy(source, buffer.at[q], sems.at[q, n])
+        half = parts[q][2].shape[0]
+        places = (
+            gate_buf.at[q],
+            up_buf.at[q],
+            down_buf.at[q, pl.ds(0, half)],
+            down_buf.at[q, pl.ds(half, half)],
+        )
+        for n, (source, place) in enumerate(zip(parts[q], places)):
+            copy = pltpu.make_async_copy(source, place, sems.at[q, n])
             copy.start()
             copies.append(copy)
     for q in range(groups):
-        copies[3 * q].wait()
+        copies[4 * q].wait()
         gate_value = jnp.dot(rows_ref[...], gate_buf[q], preferred_element_type=jnp.float32)
-        copies[3 * q + 1].wait()
+        copies[4 * q + 1].wait()
         up_value = jnp.dot(rows_ref[...], up_buf[q], preferred_element_type=jnp.float32)
         hidden = (jax.nn.silu(gate_value) * up_value).astype(jnp.bfloat16)
-        copies[3 * q + 2].wait()
+        copies[4 * q + 2].wait()
+        copies[4 * q + 3].wait()
         product = jnp.dot(hidden, down_buf[q], preferred_element_type=jnp.float32)
         if q == 0:
             total[...] = product
@@ -497,11 +498,11 @@
             out_ref[...] = ((total[...] + product) * weight_ref[...]).astype(jnp.bfloat16)
 
 
-def run_experts(rows_in, dense_weight, triples):
-    groups = len(triples)
+def run_experts(rows_in, dense_weight, parts):
+    groups = len(parts)
     count, width = rows_in.shape
-    units = triples[0][0].shape[1]
-    flat = [array for triple in triples for array in triple]
+    units = parts[0][0].shape[1]
+    flat = [array for part in parts for array in part]
     return pl.pallas_call(
         partial(experts_kernel, groups),
         out_shape=jax.ShapeDtypeStruct((count, width), jnp.bfloat16),
@@ -513,7 +514,7 @@
             pltpu.VMEM((groups, width, units), jnp.bfloat16),
             pltpu.VMEM((groups, units, width), jnp.bfloat16),
             pltpu.VMEM((count, width), jnp.float32),
-            pltpu.SemaphoreType.DMA((groups, 3)),
+            pltpu.SemaphoreType.DMA((groups, 4)),
         ],
         compiler_params=pltpu.CompilerParams(vmem_limit_bytes=40 * 1024 * 1024),
         cost_estimate=pl.CostEstimate(
@@ -550,10 +551,30 @@
     def swapped(array, step):
         return lax.ppermute(array, "tp", [(i, i ^ step) for i in range(tp)])
 
-    own = (expert_gate[0], expert_up[0], expert_down[0])
-    far = tuple(swapped(a, 2) for a in own)
-    near = tuple(swapped(a, 1) for a in own)
-    near_far = tuple(swapped(a, 1) for a in far)
+    half = expert_down.shape[1] // 2
+    own_gate, own_up = expert_gate[0], expert_up[0]
+    own_low, own_high = expert_down[0, :half], expert_down[0, half:]
+    far_residual = swapped(residual, 2)
+    far_gate = swapped(own_gate, 2)
+    far_low = swapped(own_low, 2)
+    near_residual = swapped(residual, 1)
+    near_gate, near_up, near_low, near_high = (
+        swapped(a, 1) for a in (own_gate, own_up, own_low, own_high)
+    )
+    odd, upper = t % 2 == 1, t // 2 == 1
+
+    def in_order(first, second, turned):
+        return jnp.where(
+            turned,
+            jnp.concatenate([second, first], axis=0),
+            jnp.concatenate([first, second], axis=0),
+        )
+
+    column_residual = in_order(
+        in_order(residual, near_residual, odd),
+        in_order(far_residual, swapped(far_residual, 1), odd),
+        upper,
+    )
 
     local_heads = mix_lambda.shape[0]
     head_width = head_gain.shape[0]
@@ -570,17 +591,15 @@
     lanes = -(-rows_dev // 128) * 128
     table = jnp.pad(table, ((0, 0), (0, lanes - rows_dev)))
 
-    key_all, value_all, tables = gather_sp([key_maps, value_rows, table], sp, tp, False, 1)
+    key_all, value_all = gather_sp([key_maps, value_rows], sp, tp, False, 1)
     key_all = key_all.reshape(sp * token_count, -1)
     value_all = value_all.reshape(sp * token_count, -1)
-    dense_weight = lax.dynamic_index_in_dim(tables, s, 1, False)[:, :rows_dev]
-    dense_weight = dense_weight.reshape(sp * rows_dev, 1)
 
     queries = query_maps.reshape(token_count, kv_local, head_group, 2, head_dim)
     start_max = jnp.full((kv_local, head_group, 2, token_count), lowest_score, jnp.float32)
     start_sum = jnp.zeros((kv_local, head_group, 2, token_count), jnp.float32)
     start_values = jnp.zeros((kv_local, head_group, 2, token_count, head_width), jnp.float32)
-    run_max, run_sum, accumulated = fold_keys(
+    _, run_sum, accumulated = fold_keys(
         (start_max, start_sum, start_values),
         (key_all, value_all),
         jnp.int32(0),
@@ -595,16 +614,22 @@
     attended = jnp.transpose(head_scaled, (2, 0, 1, 3)).reshape(
         token_count, local_heads * head_width
     )
-    attended = exchange_heads(attended, tp, 2)
+    attended = gather_heads(attended, tp, 2)
+    attended, late_up, late_high = lax.optimization_barrier((attended, own_up, own_high))
+    far_up = swapped(late_up, 2)
+    far_high = swapped(late_high, 2)
     projected = jnp.dot(attended, out_weight, preferred_element_type=jnp.float32)
-    stream = (residual.astype(jnp.float32) + projected).astype(jnp.bfloat16)
-    stream_wide = stream.astype(jnp.float32)
+    streams = (column_residual.astype(jnp.float32) + projected).astype(jnp.bfloat16)
+    stream_wide = streams.astype(jnp.float32)
     stream_rms = lax.rsqrt(jnp.mean(stream_wide * stream_wide, axis=1, keepdims=True) + norm_eps)
-    normed = (stream_wide * stream_rms * norm_gain).astype(jnp.bfloat16)
-
-    routed_in, shared_in = gather_sp([normed], sp, tp, True, 3)
+    shared_in = (stream_wide * stream_rms * norm_gain).astype(jnp.bfloat16)
+    stream = lax.dynamic_slice_in_dim(streams, t * rows_dev, rows_dev, 0)
+    normed = lax.dynamic_slice_in_dim(shared_in, t * rows_dev, rows_dev, 0)
+
+    routed_in, tables = gather_sp([normed, table], sp, tp, False, 3)
+    dense_weight = lax.dynamic_index_in_dim(tables, s, 1, False)[:, :rows_dev]
+    dense_weight = dense_weight.reshape(sp * rows_dev, 1)
     width = normed.shape[1]
-    shared_in = shared_in.reshape(tp * rows_dev, width)
     shared_hidden = (
         jax.nn.silu(jnp.dot(shared_in, shared_gate, preferred_element_type=jnp.float32))
         * jnp.dot(shared_in, shared_up, preferred_element_type=jnp.float32)
@@ -612,8 +637,16 @@
     shared_out = jnp.dot(shared_hidden, shared_down, preferred_element_type=jnp.float32)
     shared_out = shared_out.astype(jnp.bfloat16).reshape(tp, rows_dev, width)
 
+    near_far = tuple(swapped(a, 1) for a in (far_gate, far_up, far_low, far_high))
     routed = run_experts(
-        routed_in.reshape(sp * rows_dev, width), dense_weight, (own, near, far, near_far)
+        routed_in.reshape(sp * rows_dev, width),
+        dense_weight,
+        (
+            (own_gate, own_up, own_low, own_high),
+            (near_gate, near_up, near_low, near_high),
+            (far_gate, far_up, far_low, far_high),
+            near_far,
+        ),
     )
     return return_rows(routed.reshape(sp, rows_dev, width), shared_out, stream, sp, tp, 4)
 
@@ -646,7 +679,9 @@
         rows_dev = args[6].shape[0]
         whole_blocks = 2 * rows_dev * route_count >= experts * rows_dev
         dense = whole_blocks and args[10].shape[0] == 1 and sp == 8 and tp == 4
-        return (dense_body if dense else body)(*args)
+        if not dense:
+            return body(*args)
+        return dense_body(*args)
 
     return jax.shard_map(
         chosen, mesh=mesh, in_specs=in_specs, out_specs=out_specs, check_vma=False

time: 165 us -> 194 us (1.18)
  waiting for transfers between devices: 0.02 us -> 47.4 us
  Pallas kernels: 131 us -> 107 us
  starting transfers between devices: 6.34 us -> 8.31 us
    ppermute x9 -> x15, waiting for transfers between devices: 0.02 us -> 47.4 us  [swapped(): return lax.ppermute(array, 'tp', [(i, i ^ step) for i in range(tp)])]
    pallas_call x1, Pallas kernels: 35.5 us -> 7.98 us  [gather_heads(): pl.pallas_call(partial(heads_kernel, tp), out_shape=jax.ShapeDtypeStruct(...]
    pallas_call x1, Pallas kernels: 27.1 us -> 31.2 us  [return_rows(): pl.pallas_call(partial(return_kernel, sp, tp), out_shape=jax.ShapeDtypeSt...]
    select_n x0 -> x2, other arithmetic: none -> 2.42 us  [in_order(): jnp.where(turned, jnp.concatenate([second, first], axis=0), jnp.concatena...]
    dynamic_slice x0 -> x2, local copies, waits for them, and re-layouts: none -> 2.32 us  [the longest x1 1.62 us: dense_body(): stream = lax.dynamic_slice_in_dim(streams, t * rows_dev, rows_dev, 0)]
    ppermute x9 -> x15, starting transfers between devices: 6.34 us -> 8.31 us  [swapped(): return lax.ppermute(array, 'tp', [(i, i ^ step) for i in range(tp)])]
    unnamed x26 -> x32, local copies, waits for them, and re-layouts: 6.67 us -> 5.46 us
  transfers between devices with their start and end apart: 9 -> 15, of which waited for: 0 -> 5; matrix products, arithmetic and copies ran while one was open for 14% -> 13% of each run, Pallas kernels for 56% -> 33%
where the time goes in v2:
time: 194 us; the launch traced here: 193 us
  Pallas kernels  107 us (55%)
  waiting for transfers between devices  47.4 us (24%)
  local copies, waits for them, and re-layouts  13.9 us (7%)
  matrix products  11.4 us (6%)
  starting transfers between devices  8.31 us (4%)
  other arithmetic  4.66 us (2%)
    pallas_call x2, Pallas kernels, gather_sp(): pl.pallas_call(partial(gather_kernel, sp, tp, count, with_tp), out_shape=...  56.2 us
    ppermute x15, waiting for transfers between devices, swapped(): return lax.ppermute(array, 'tp', [(i, i ^ step) for i in range(tp)])  47.4 us
    pallas_call x1, Pallas kernels, return_rows(): pl.pallas_call(partial(return_kernel, sp, tp), out_shape=jax.ShapeDtypeSt...  31.2 us
    pallas_call x1, Pallas kernels, run_experts(): pl.pallas_call(partial(experts_kernel, groups), out_shape=jax.ShapeDtypeS...  11.9 us
    ppermute x15, starting transfers between devices, swapped(): return lax.ppermute(array, 'tp', [(i, i ^ step) for i in range(tp)])  8.31 us
    pallas_call x1, Pallas kernels, gather_heads(): pl.pallas_call(partial(heads_kernel, tp), out_shape=jax.ShapeDtypeStruct(...  7.98 us
    unnamed x32, local copies, waits for them, and re-layouts  5.46 us
  transfers between devices with their start and end apart: 15, of which 5 were waited for; matrix products, arithmetic and copies ran while one was open for 13% of the time, Pallas kernels for 33%

profile of v2, /device:TPU:0, one launch (start us, length us, event | category | flops | bytes accessed | tf_op | source)
XLA Modules:
  0.0 193.5 jit_solution(6795101002913019109)
XLA Ops:
  0.0 3.0 %collective-permute-start = (bf16[48,2048]{1,0:T(8,128)(2,1)}, bf16[48,2048]{1,0:T(8,128)(2,1)}, u32[]{:S(2)}, u32[]{:S(2)}) collective-permute-start(bf16[48,2048]{1,0:T(8,128)(2,1)} %param.24), channel_id=1, source_target_pairs={{0,2},{1,3},{2,0},{3,1},{4,6},{5,7},{6,4},{7,5},{8,10},{9,11},{10,... | collective-permute-start | bytes 589832 | tf_op jit(solution)/shard_map/ppermute | solution.py:552
  3.0 1.3 slice_bitcast_fusion
  4.3 0.2 collective-permute-start.9
  4.5 0.4 collective-permute-start.5
  5.1 20.2 %shard_map.154 = (bf16[8,192,128]{2,1,0:T(8,128)(2,1)}, bf16[8,192,128]{2,1,0:T(8,128)(2,1)S(1)}) custom-call(bf16[192,128]{1,0:T(8,128)(2,1)} %refs_0_.1, bf16[192,128]{1,0:T(8,128)(2,1)} %refs_1_.1), custom_call_target="tpu_custom_call" | custom-call | bytes 40000000 | tf_op jit(solution)/shard_map/pallas_call | solution.py:317
  25.4 7.5 %while.18 = (s32[]{:T(128)}, f32[1,2,2,192]{3,1,2,0:T(2,128)S(1)}, f32[1,2,2,192]{3,1,2,0:T(2,128)S(1)}, f32[1,2,2,192,128]{4,3,2,1,0:T(8,128)S(1)}, bf16[1536,1...) while((s32[]{:T(128)}, f32[1,2,2,192]{3,1,2,0:T(2,128)S(1)}, ...), condition=%wide.region_3.4_spmd.clone, body=%wide.region_0.3_spmd.clone.sunk | while | flops 153260544 | bytes 6443191 | solution.py:78
  25.4 0.9 constant_dynamic-slice_fusion.6
  26.4 0.5 bitcast_reduce_fusion.2
  27.0 0.5 fusion.45
  27.5 0.4 fusion.46
  27.9 0.9 constant_dynamic-slice_fusion.6
  28.9 0.5 bitcast_reduce_fusion.2
  29.5 0.5 fusion.45
  30.0 0.4 fusion.46
  30.4 0.9 constant_dynamic-slice_fusion.6
  31.4 0.5 bitcast_reduce_fusion.2
  32.0 0.5 fusion.45
  32.5 0.4 fusion.46
  32.9 0.2 broadcast_divide_fusion
  33.1 0.2 multiply_reduce_fusion
  33.6 0.7 copy.53
  34.2 8.0 %shard_map.155 = bf16[192,1024]{1,0:T(8,128)(2,1)} custom-call(bf16[192,256]{1,0:T(8,128)(2,1)} %bitcast.126), custom_call_target="tpu_custom_call" | custom-call | bytes 20000000 | tf_op jit(solution)/shard_map/pallas_call | solution.py:357
  42.2 1.0 collective-permute-start.10
  43.3 0.6 pad.4.refs_1_
  43.9 1.1 collective-permute-start.8
  45.0 0.2 collective-permute-start.1
  45.2 1.3 maximum_select_fusion.2
  46.7 1.5 collective-permute-start.7
  48.2 1.1 maximum_select_fusion.1
  49.3 3.4 %fusion.12 = (f32[192]{0:T(256)S(1)}, bf16[192,2048]{1,0:T(8,128)(2,1)S(1)}) fusion(bf16[192,1024]{1,0:T(8,128)(2,1)S(1)} %copy-done.7, bf16[1024,2048]{1,0:T(8,128)(2,1)} %param.23, bf16[96,2048]{1,0:T(8,128)(2,1)S(1)} %maximum_select_fusion.1, bf16[96,2048]{1,0:T(8,128)(2,1)S(1)} %maximum_select_fusion.2, pred[]{:T(512)S(6)} %eq.21), kind=kOutput, calls=%fused_computation.27 | convolution fusion | flops 811204416 | bytes 6161153 | tf_op jit(solution)/shard_map/dot_general | solution.py:621
  52.7 4.5 %collective-permute-done.10.refs_13_ = bf16[128,2048]{1,0:T(8,128)(2,1)} collective-permute-done((bf16[128,2048]{1,0:T(8,128)(2,1)S(1)}, bf16[128,2048]{1,0:T(8,128)(2,1)}, u32[]{:S(2)}, u32[]{:S(2)}) %collective-permute-start.10) | collective-permute-done | bytes 524320 | tf_op jit(solution)/shard_map/ppermute | solution.py:552
  57.2 0.3 fusion.14
  57.5 0.6 collective-permute-start.3
  58.1 1.0 collective-permute-done.6.refs_9_
  59.1 0.8 copy-done.3
  60.1 19.6 %collective-permute-done.8.refs_11_ = bf16[2048,256]{1,0:T(8,128)(2,1)} collective-permute-done((bf16[2048,256]{1,0:T(8,128)(2,1)}, bf16[2048,256]{1,0:T(8,128)(2,1)}, u32[]{:S(2)}, u32[]{:S(2)}) %collective-permute-start.8) | collective-permute-done | bytes 1048608 | tf_op jit(solution)/shard_map/ppermute | solution.py:552
  79.7 22.3 %collective-permute-done.7.refs_10_ = bf16[2048,256]{1,0:T(8,128)(2,1)} collective-permute-done((bf16[2048,256]{1,0:T(8,128)(2,1)S(1)}, bf16[2048,256]{1,0:T(8,128)(2,1)}, u32[]{:S(2)}, u32[]{:S(2)}) %collective-permute-start.7) | collective-permute-done | bytes 1048608 | tf_op jit(solution)/shard_map/ppermute | solution.py:552
  101.9 0.7 constant_dynamic-slice_fusion.4.refs_0_
  102.6 36.0 %shard_map.156 = (bf16[8,48,2048]{2,1,0:T(8,128)(2,1)}, f32[8,8,128]{2,1,0:T(8,128)}) custom-call(bf16[48,2048]{1,0:T(8,128)(2,1)} %constant_dynamic-slice_fusion.4.refs_0_, f32[8,128]{1,0:T(8,128)} %pad.4.refs_1_), custom_call_target="tpu_custom_call" | custom-call | bytes 40000000 | tf_op jit(solution)/shard_map/pallas_call | solution.py:317
  138.6 0.8 constant_dynamic-slice_fusion.2
  139.5 1.8 fusion.26
  141.5 1.6 constant_dynamic-slice_fusion.1.stream_ref
  143.1 3.4 %convolution_convert_fusion = bf16[192,2048]{1,0:T(8,128)(2,1)} fusion(bf16[256,2048]{1,0:T(8,128)(2,1)S(1)} %copy-done, bf16[192,2048]{1,0:T(8,128)(2,1)} %copy-done.5, bf16[2048,256]{1,0:T(8,128)(2,1)} %param.32, f32[192,256]{1,0:T(8,128)S(1)} %fusion.26), kind=kOutput, calls=%fused_computation.24 | convolution fusion | flops 403341312 | bytes 3866624 | tf_op jit(solution)/shard_map/dot_general | solution.py:637
  146.6 1.0 copy-done.4
  147.6 11.9 %shard_map.157 = bf16[384,2048]{1,0:T(8,128)(2,1)S(1)} custom-call(bf16[384,2048]{1,0:T(8,128)(2,1)} %bitcast.129, f32[384,1]{1,0:T(8,128)S(1)} %reshape.167.refs_1_, bf16[2048,256]{1,0:T(8,128)(2,1)S(1)} %bitcast.118, bf16[2048,256]{1,0:T(8,128)(2,1)} %bitcast.7.refs_3_, bf16[128,2048]{1,0:T(8,128)(2,1)S(1)} %get-tuple-element.211.refs_4_, ...), custom_call_target="tpu_custom_call" | custom-call | flops 4831838208 | bytes 12000000 | tf_op jit(solution)/shard_map/pallas_call | solution.py:506
  159.5 1.2 copy-done.1
  160.7 31.2 %shard_map.158 = bf16[48,2048]{1,0:T(8,128)(2,1)} custom-call(bf16[8,48,2048]{2,1,0:T(8,128)(2,1)} %bitcast.115, bf16[4,48,2048]{2,1,0:T(8,128)(2,1)} %bitcast.120, bf16[48,2048]{1,0:T(8,128)(2,1)} %constant_dynamic-slice_fusion.1.stream_ref), custom_call_target="tpu_custom_call" | custom-call | bytes 60000000 | tf_op jit(solution)/shard_map/pallas_call | solution.py:447
  191.9 1.6 copy.73
  (71 shorter events, 1.5 us)
Async XLA Ops:
  0.0 143.1 %copy-start = (bf16[256,2048]{1,0:T(8,128)(2,1)S(1)}, bf16[256,2048]{1,0:T(8,128)(2,1)}, u32[]{:S(2)}) copy-start(bf16[256,2048]{1,0:T(8,128)(2,1)} %param.33) | copy-start | bytes 3145732
  0.0 5.0 %copy-start.8 = (bf16[192,256]{1,0:T(8,128)(2,1)S(1)}, bf16[192,256]{1,0:T(8,128)(2,1)}, u32[]{:S(2)}) copy-start(bf16[192,256]{1,0:T(8,128)(2,1)} %param.18) | copy-start | bytes 294916
  0.0 43.9 %collective-permute-start = (bf16[48,2048]{1,0:T(8,128)(2,1)}, bf16[48,2048]{1,0:T(8,128)(2,1)}, u32[]{:S(2)}, u32[]{:S(2)}) collective-permute-start(bf16[48,2048]{1,0:T(8,128)(2,1)} %param.24), channel_id=1, source_target_pairs={{0,2},{1,3},{2,0},{3,1},{4,6},{5,7},{6,4},{7,5},{8,10},{9,11},{10,... | collective-permute-start | bytes 589832 | tf_op jit(solution)/shard_map/ppermute | solution.py:552
  3.0 42.0 %collective-permute-start.2 = (bf16[48,2048]{1,0:T(8,128)(2,1)}, bf16[48,2048]{1,0:T(8,128)(2,1)}, u32[]{:S(2)}, u32[]{:S(2)}) collective-permute-start(bf16[48,2048]{1,0:T(8,128)(2,1)} %param.24), channel_id=1, source_target_pairs={{0,1},{1,0},{2,3},{3,2},{4,5},{5,4},{6,7},{7,6},{8,9},{9,8},{10,11... | collective-permute-start | bytes 589832 | tf_op jit(solution)/shard_map/ppermute | solution.py:552
  4.3 53.2 %collective-permute-start.9 = (bf16[128,2048]{1,0:T(8,128)(2,1)S(1)}, bf16[128,2048]{1,0:T(8,128)(2,1)}, u32[]{:S(2)}, u32[]{:S(2)}) collective-permute-start(bf16[128,2048]{1,0:T(8,128)(2,1)S(1)} %get-tuple-element.211.refs_4_), channel_id=1, source_target_pairs={{0,2},{1,3},{2,0},{3,1},{4,6},{5,7},{6,4},{7,5},{8,10},{9,11},{10,... | collective-permute-start | bytes 1572872 | tf_op jit(solution)/shard_map/ppermute | solution.py:552
  4.5 53.5 %collective-permute-start.5 = (bf16[128,2048]{1,0:T(8,128)(2,1)S(1)}, bf16[128,2048]{1,0:T(8,128)(2,1)}, u32[]{:S(2)}, u32[]{:S(2)}) collective-permute-start(bf16[128,2048]{1,0:T(8,128)(2,1)S(1)} %get-tuple-element.211.refs_4_), channel_id=1, source_target_pairs={{0,1},{1,0},{2,3},{3,2},{4,5},{5,4},{6,7},{7,6},{8,9},{9,8},{10,11... | collective-permute-start | bytes 1572872 | tf_op jit(solution)/shard_map/ppermute | solution.py:552
  25.3 7.8 %copy-start.11 = (f32[2]{0:T(128)S(1)}, f32[2]{0:T(128)}, u32[]{:S(2)}) copy-start(f32[2]{0:T(128)} %param.21) | copy-start | bytes 28
  25.4 8.0 %copy-start.13 = (f32[128]{0:T(128)S(1)}, f32[128]{0:T(128)}, u32[]{:S(2)}) copy-start(f32[128]{0:T(128)} %param.22) | copy-start | bytes 1540
  32.9 10.4 %copy-start.12 = (s32[192,4]{0,1:T(4,128)S(1)}, s32[192,4]{0,1:T(4,128)}, u32[]{:S(2)}) copy-start(s32[192,4]{0,1:T(4,128)} %param.26) | copy-start | bytes 9220
  32.9 10.4 %copy-start.10 = (f32[48,4]{0,1:T(4,128)S(1)}, f32[48,4]{0,1:T(4,128)}, u32[]{:S(2)}) copy-start(f32[48,4]{0,1:T(4,128)} %param.27) | copy-start | bytes 2308
  32.9 13.8 %copy-start.2 = (bf16[1,2048,256]{2,1,0:T(8,128)(2,1)S(1)}, bf16[1,2048,256]{2,1,0:T(8,128)(2,1)}, u32[]{:S(2)}) copy-start(bf16[1,2048,256]{2,1,0:T(8,128)(2,1)} %param.28) | copy-start | bytes 3145732
  42.2 7.1 %copy-start.7 = (bf16[192,1024]{1,0:T(8,128)(2,1)S(1)}, bf16[192,1024]{1,0:T(8,128)(2,1)}, u32[]{:S(2)}) copy-start(bf16[192,1024]{1,0:T(8,128)(2,1)} %shard_map.155) | copy-start | bytes 1179652
  42.2 15.0 %collective-permute-start.10 = (bf16[128,2048]{1,0:T(8,128)(2,1)S(1)}, bf16[128,2048]{1,0:T(8,128)(2,1)}, u32[]{:S(2)}, u32[]{:S(2)}) collective-permute-start(bf16[128,2048]{1,0:T(8,128)(2,1)S(1)} %get-tuple-element.145.refs_5_), channel_id=1, source_target_pairs={{0,2},{1,3},{2,0},{3,1},{4,6},{5,7},{6,4},{7,5},{8,10},{9,11},{10,... | collective-permute-start | bytes 1572872 | tf_op jit(solution)/shard_map/ppermute | solution.py:552
  43.9 35.7 %collective-permute-start.8 = (bf16[2048,256]{1,0:T(8,128)(2,1)}, bf16[2048,256]{1,0:T(8,128)(2,1)}, u32[]{:S(2)}, u32[]{:S(2)}) collective-permute-start(bf16[2048,256]{1,0:T(8,128)(2,1)} %bitcast.7.refs_3_), channel_id=1, source_target_pairs={{0,2},{1,3},{2,0},{3,1},{4,6},{5,7},{6,4},{7,5},{8,10},{9,11},{10,... | collective-permute-start | bytes 3145736 | tf_op jit(solution)/shard_map/ppermute | solution.py:552
  45.0 1.7 collective-permute-start.1
  46.7 55.3 %collective-permute-start.7 = (bf16[2048,256]{1,0:T(8,128)(2,1)S(1)}, bf16[2048,256]{1,0:T(8,128)(2,1)}, u32[]{:S(2)}, u32[]{:S(2)}) collective-permute-start(bf16[2048,256]{1,0:T(8,128)(2,1)S(1)} %bitcast.116), channel_id=1, source_target_pairs={{0,2},{1,3},{2,0},{3,1},{4,6},{5,7},{6,4},{7,5},{8,10},{9,11},{10,... | collective-permute-start | bytes 3145736 | tf_op jit(solution)/shard_map/ppermute | solution.py:552
  49.3 7.9 %copy-start.9 = (f32[2048]{0:T(1024)S(1)}, f32[2048]{0:T(1024)}, u32[]{:S(2)}) copy-start(f32[2048]{0:T(1024)} %param.25) | copy-start | bytes 24580
  52.7 49.2 %copy-start.6 = (bf16[192,2048]{1,0:T(8,128)(2,1)}, bf16[192,2048]{1,0:T(8,128)(2,1)S(1)}, u32[]{:S(2)}) copy-start(bf16[192,2048]{1,0:T(8,128)(2,1)S(1)} %get-tuple-element.214) | copy-start | bytes 2359300
  57.2 1.9 collective-permute-start.6
  57.5 44.5 %copy-start.5 = (bf16[192,2048]{1,0:T(8,128)(2,1)}, bf16[192,2048]{1,0:T(8,128)(2,1)S(1)}, u32[]{:S(2)}) copy-start(bf16[192,2048]{1,0:T(8,128)(2,1)S(1)} %fusion.14) | copy-start | bytes 2359300
  57.5 89.1 %collective-permute-start.3 = (bf16[2048,256]{1,0:T(8,128)(2,1)S(1)}, bf16[2048,256]{1,0:T(8,128)(2,1)}, u32[]{:S(2)}, u32[]{:S(2)}) collective-permute-start(bf16[2048,256]{1,0:T(8,128)(2,1)S(1)} %bitcast.117), channel_id=1, source_target_pairs={{0,1},{1,0},{2,3},{3,2},{4,5},{5,4},{6,7},{7,6},{8,9},{9,8},{10,11... | collective-permute-start | bytes 3145736 | tf_op jit(solution)/shard_map/ppermute | solution.py:552
  58.1 88.5 %collective-permute-start.4 = (bf16[2048,256]{1,0:T(8,128)(2,1)}, bf16[2048,256]{1,0:T(8,128)(2,1)}, u32[]{:S(2)}, u32[]{:S(2)}) collective-permute-start(bf16[2048,256]{1,0:T(8,128)(2,1)} %bitcast.7.refs_3_), channel_id=1, source_target_pairs={{0,1},{1,0},{2,3},{3,2},{4,5},{5,4},{6,7},{7,6},{8,9},{9,8},{10,11... | collective-permute-start | bytes 3145736 | tf_op jit(solution)/shard_map/ppermute | solution.py:552
  59.1 0.8 copy-start.3
  59.9 81.5 %collective-permute-start.14 = (bf16[128,2048]{1,0:T(8,128)(2,1)}, bf16[128,2048]{1,0:T(8,128)(2,1)}, u32[]{:S(2)}, u32[]{:S(2)}) collective-permute-start(bf16[128,2048]{1,0:T(8,128)(2,1)} %collective-permute-done.10.refs_13_), channel_id=1, source_target_pairs={{0,1},{1,0},{2,3},{3,2},{4,5},{5,4},{6,7},{7,6},{8,9},{9,8},{10,11... | collective-permute-start | bytes 1572872 | tf_op jit(solution)/shard_map/ppermute | solution.py:552
  79.7 66.9 %collective-permute-start.12 = (bf16[2048,256]{1,0:T(8,128)(2,1)}, bf16[2048,256]{1,0:T(8,128)(2,1)}, u32[]{:S(2)}, u32[]{:S(2)}) collective-permute-start(bf16[2048,256]{1,0:T(8,128)(2,1)} %collective-permute-done.8.refs_11_), channel_id=1, source_target_pairs={{0,1},{1,0},{2,3},{3,2},{4,5},{5,4},{6,7},{7,6},{8,9},{9,8},{10,11... | collective-permute-start | bytes 3145736 | tf_op jit(solution)/shard_map/ppermute | solution.py:552
  101.9 44.6 %collective-permute-start.11 = (bf16[2048,256]{1,0:T(8,128)(2,1)}, bf16[2048,256]{1,0:T(8,128)(2,1)}, u32[]{:S(2)}, u32[]{:S(2)}) collective-permute-start(bf16[2048,256]{1,0:T(8,128)(2,1)} %collective-permute-done.7.refs_10_), channel_id=1, source_target_pairs={{0,1},{1,0},{2,3},{3,2},{4,5},{5,4},{6,7},{7,6},{8,9},{9,8},{10,11... | collective-permute-start | bytes 3145736 | tf_op jit(solution)/shard_map/ppermute | solution.py:552
  141.4 5.2 %collective-permute-start.13 = (bf16[128,2048]{1,0:T(8,128)(2,1)}, bf16[128,2048]{1,0:T(8,128)(2,1)}, u32[]{:S(2)}, u32[]{:S(2)}) collective-permute-start(bf16[128,2048]{1,0:T(8,128)(2,1)} %collective-permute-done.9.refs_12_), channel_id=1, source_target_pairs={{0,1},{1,0},{2,3},{3,2},{4,5},{5,4},{6,7},{7,6},{8,9},{9,8},{10,11... | collective-permute-start | bytes 1572872 | tf_op jit(solution)/shard_map/ppermute | solution.py:552
  146.6 1.0 copy-start.4
  159.5 1.2 copy-start.1

commit v3 on v2

--- a/solution.py
+++ b/solution.py
@@ -248,7 +248,7 @@
     copies = []
     arrivals = []
     for i in range(count):
-        for k in range(depth - 1, 0, -1):
+        for k in (1, 3, 2) if depth == 4 else range(1, depth):
             copy = remote(
                 ins[i], outs[i].at[s], send_sem.at[i, k], recv_sem.at[i, k], line[k - 1]
             )
@@ -325,7 +325,9 @@
             pltpu.SemaphoreType.DMA((count + 1,)),
         ],
         compiler_params=pltpu.CompilerParams(
-            collective_id=collective_id, has_side_effects=True
+            collective_id=collective_id,
+            has_side_effects=True,
+            vmem_limit_bytes=16 * 1024 * 1024,
         ),
         cost_estimate=pl.CostEstimate(flops=0, bytes_accessed=40_000_000, transcendentals=0),
     )(*arrays)
@@ -365,7 +367,9 @@
             pltpu.SemaphoreType.DMA,
         ],
         compiler_params=pltpu.CompilerParams(
-            collective_id=collective_id, has_side_effects=True
+            collective_id=collective_id,
+            has_side_effects=True,
+            vmem_limit_bytes=16 * 1024 * 1024,
         ),
         cost_estimate=pl.CostEstimate(flops=0, bytes_accessed=20_000_000, transcendentals=0),
     )(attended)
@@ -458,7 +462,9 @@
             pltpu.SemaphoreType.DMA((slots,)),
         ],
         compiler_params=pltpu.CompilerParams(
-            collective_id=collective_id, has_side_effects=True
+            collective_id=collective_id,
+            has_side_effects=True,
+            vmem_limit_bytes=16 * 1024 * 1024,
         ),
         cost_estimate=pl.CostEstimate(flops=0, bytes_accessed=60_000_000, transcendentals=0),
     )(routed, shared, stream)

time: 194 us -> 182 us (0.938)
  Pallas kernels: 107 us -> 94.9 us
  local copies, waits for them, and re-layouts: 13.9 us -> 11.5 us
    pallas_call x2, Pallas kernels: 56.2 us -> 47.4 us  [gather_sp(): pl.pallas_call(partial(gather_kernel, sp, tp, count, with_tp), out_shape=...]
    pallas_call x1, Pallas kernels: 31.2 us -> 28.4 us  [return_rows(): pl.pallas_call(partial(return_kernel, sp, tp), out_shape=jax.ShapeDtypeSt...]
    dot_general x3, matrix products: 1.13 us -> 3.84 us  [attention_block(): jnp.einsum('agcqr,rae->agcqe', weights.astype(jnp.bfloat16), value_heads,...]
    unnamed x32 -> x34, local copies, waits for them, and re-layouts: 5.46 us -> 4.9 us
  transfers between devices with their start and end apart: 15 -> 15, of which waited for: 5 -> 5; matrix products, arithmetic and copies ran while one was open for 13% -> 14% of each run, Pallas kernels for 33% -> 30%
where the time goes in v3:
time: 182 us; the launch traced here: 181 us
  Pallas kernels  94.9 us (52%)
  waiting for transfers between devices  47 us (26%)
  matrix products  13.2 us (7%)
  local copies, waits for them, and re-layouts  11.5 us (6%)
  starting transfers between devices  8.54 us (5%)
  other arithmetic  5.58 us (3%)
    pallas_call x2, Pallas kernels, gather_sp(): pl.pallas_call(partial(gather_kernel, sp, tp, count, with_tp), out_shape=...  47.4 us
    ppermute x15, waiting for transfers between devices, swapped(): return lax.ppermute(array, 'tp', [(i, i ^ step) for i in range(tp)])  47 us
    pallas_call x1, Pallas kernels, return_rows(): pl.pallas_call(partial(return_kernel, sp, tp), out_shape=jax.ShapeDtypeSt...  28.4 us
    pallas_call x1, Pallas kernels, run_experts(): pl.pallas_call(partial(experts_kernel, groups), out_shape=jax.ShapeDtypeS...  12.7 us
    ppermute x15, starting transfers between devices, swapped(): return lax.ppermute(array, 'tp', [(i, i ^ step) for i in range(tp)])  8.54 us
    pallas_call x1, Pallas kernels, gather_heads(): pl.pallas_call(partial(heads_kernel, tp), out_shape=jax.ShapeDtypeStruct(...  6.37 us
    unnamed x34, local copies, waits for them, and re-layouts  4.9 us
    dot_general x3, matrix products, attention_block(): jnp.einsum('agcqr,rae->agcqe', weights.astype(jnp.bfloat16), value_heads,...  3.84 us
  transfers between devices with their start and end apart: 15, of which 5 were waited for; matrix products, arithmetic and copies ran while one was open for 14% of the time, Pallas kernels for 30%

profile of v3, /device:TPU:0, one launch (start us, length us, event | category | flops | bytes accessed | tf_op | source)
XLA Modules:
  0.0 181.2 jit_solution(14362973164232723225)
XLA Ops:
  0.0 3.1 %collective-permute-start = (bf16[48,2048]{1,0:T(8,128)(2,1)}, bf16[48,2048]{1,0:T(8,128)(2,1)}, u32[]{:S(2)}, u32[]{:S(2)}) collective-permute-start(bf16[48,2048]{1,0:T(8,128)(2,1)} %param.24), channel_id=1, source_target_pairs={{0,2},{1,3},{2,0},{3,1},{4,6},{5,7},{6,4},{7,5},{8,10},{9,11},{10,... | collective-permute-start | bytes 589832 | tf_op jit(solution)/shard_map/ppermute | solution.py:558
  3.1 1.3 slice_bitcast_fusion
  4.4 0.2 collective-permute-start.9
  4.6 0.4 collective-permute-start.5
  5.2 18.5 %shard_map.154 = (bf16[8,192,128]{2,1,0:T(8,128)(2,1)}, bf16[8,192,128]{2,1,0:T(8,128)(2,1)}) custom-call(bf16[192,128]{1,0:T(8,128)(2,1)S(1)} %copy-done.1, bf16[192,128]{1,0:T(8,128)(2,1)S(1)} %copy-done.2), custom_call_target="tpu_custom_call" | custom-call | bytes 40000000 | tf_op jit(solution)/shard_map/pallas_call | solution.py:317
  23.7 10.2 %while.18 = (s32[]{:T(128)}, f32[1,2,2,192]{3,1,2,0:T(2,128)S(1)}, f32[1,2,2,192]{3,1,2,0:T(2,128)S(1)}, f32[1,2,2,192,128]{4,3,2,1,0:T(8,128)S(1)}, bf16[1536,1...) while((s32[]{:T(128)}, f32[1,2,2,192]{3,1,2,0:T(2,128)S(1)}, ...), condition=%wide.region_3.4_spmd.clone, body=%wide.region_0.3_spmd.clone.sunk | while | flops 153260544 | bytes 6442167 | solution.py:78
  23.7 0.9 constant_dynamic-slice_fusion.6
  24.8 0.5 bitcast_reduce_fusion.2
  25.3 0.5 fusion.45
  25.8 1.3 fusion.46
  27.1 0.9 constant_dynamic-slice_fusion.6
  28.2 0.5 bitcast_reduce_fusion.2
  28.7 0.5 fusion.45
  29.2 1.3 fusion.46
  30.5 0.9 constant_dynamic-slice_fusion.6
  31.6 0.5 bitcast_reduce_fusion.2
  32.1 0.5 fusion.45
  32.6 1.3 fusion.46
  34.0 0.2 broadcast_divide_fusion
  34.2 0.2 multiply_reduce_fusion
  34.4 0.1 fusion.23
  34.6 6.4 %shard_map.155 = bf16[192,1024]{1,0:T(8,128)(2,1)S(1)} custom-call(bf16[192,256]{1,0:T(8,128)(2,1)S(1)} %bitcast.117), custom_call_target="tpu_custom_call" | custom-call | bytes 20000000 | tf_op jit(solution)/shard_map/pallas_call | solution.py:359
  41.0 1.0 collective-permute-start.10
  42.1 1.2 collective-permute-start.8
  43.3 0.2 collective-permute-start.1
  43.5 1.3 maximum_select_fusion.2
  45.0 1.5 collective-permute-start.7
  46.4 1.1 maximum_select_fusion.1
  47.6 3.4 %fusion.12 = (f32[192]{0:T(256)S(1)}, bf16[192,2048]{1,0:T(8,128)(2,1)S(1)}) fusion(bf16[192,1024]{1,0:T(8,128)(2,1)S(1)} %shard_map.155, bf16[1024,2048]{1,0:T(8,128)(2,1)} %param.23, bf16[96,2048]{1,0:T(8,128)(2,1)S(1)} %maximum_select_fusion.1, bf16[96,2048]{1,0:T(8,128)(2,1)S(1)} %maximum_select_fusion.2, pred[]{:T(512)S(6)} %eq.21), kind=kOutput, calls=%fused_computation.27 | convolution fusion | flops 811204416 | bytes 6161153 | tf_op jit(solution)/shard_map/dot_general | solution.py:627
  51.0 4.9 %collective-permute-done.10.refs_13_ = bf16[128,2048]{1,0:T(8,128)(2,1)S(1)} collective-permute-done((bf16[128,2048]{1,0:T(8,128)(2,1)S(1)}, bf16[128,2048]{1,0:T(8,128)(2,1)S(1)}, u32[]{:S(2)}, u32[]{:S(2)}) %collective-permute-start.10) | collective-permute-done | bytes 524320 | tf_op jit(solution)/shard_map/ppermute | solution.py:558
  55.9 1.2 fusion.14
  57.1 0.5 collective-permute-start.3
  57.7 0.1 collective-permute-done.6.refs_9_
  57.8 0.8 copy-done.6
  58.6 0.3 collective-permute-start.14
  58.9 19.5 %collective-permute-done.8.refs_11_ = bf16[2048,256]{1,0:T(8,128)(2,1)} collective-permute-done((bf16[2048,256]{1,0:T(8,128)(2,1)}, bf16[2048,256]{1,0:T(8,128)(2,1)}, u32[]{:S(2)}, u32[]{:S(2)}) %collective-permute-start.8) | collective-permute-done | bytes 1048608 | tf_op jit(solution)/shard_map/ppermute | solution.py:558
  78.5 22.3 %collective-permute-done.7.refs_10_ = bf16[2048,256]{1,0:T(8,128)(2,1)} collective-permute-done((bf16[2048,256]{1,0:T(8,128)(2,1)}, bf16[2048,256]{1,0:T(8,128)(2,1)}, u32[]{:S(2)}, u32[]{:S(2)}) %collective-permute-start.7) | collective-permute-done | bytes 1048608 | tf_op jit(solution)/shard_map/ppermute | solution.py:558
  100.8 0.9 constant_dynamic-slice_fusion.4.refs_0_
  101.7 28.9 %shard_map.156 = (bf16[8,48,2048]{2,1,0:T(8,128)(2,1)S(1)}, f32[8,8,128]{2,1,0:T(8,128)S(1)}) custom-call(bf16[48,2048]{1,0:T(8,128)(2,1)S(1)} %constant_dynamic-slice_fusion.4.refs_0_, f32[8,128]{1,0:T(8,128)S(1)} %pad.4.refs_1_), custom_call_target="tpu_custom_call" | custom-call | bytes 40000000 | tf_op jit(solution)/shard_map/pallas_call | solution.py:317
  130.6 1.2 copy-done.3
  131.9 1.8 %fusion.26 = f32[192,256]{1,0:T(8,128)S(1)} fusion(bf16[192,2048]{1,0:T(8,128)(2,1)} %fusion.14, bf16[2048,256]{1,0:T(8,128)(2,1)} %param.31), kind=kOutput, calls=%fused_computation.61 | convolution fusion | flops 201326592 | bytes 2031616 | tf_op jit(solution)/shard_map/dot_general | solution.py:640
  133.8 0.9 constant_dynamic-slice_fusion.1.stream_ref
  134.8 2.5 %convolution_convert_fusion = bf16[192,2048]{1,0:T(8,128)(2,1)S(1)} fusion(bf16[256,2048]{1,0:T(8,128)(2,1)S(1)} %copy-done, bf16[192,2048]{1,0:T(8,128)(2,1)} %fusion.14, bf16[2048,256]{1,0:T(8,128)(2,1)} %param.32, f32[192,256]{1,0:T(8,128)S(1)} %fusion.26), kind=kOutput, calls=%fused_computation.24 | convolution fusion | flops 403341312 | bytes 3866624 | tf_op jit(solution)/shard_map/dot_general | solution.py:643
  137.4 1.0 copy-done.5
  138.4 1.0 copy-done.7
  139.4 12.7 %shard_map.157 = bf16[384,2048]{1,0:T(8,128)(2,1)S(1)} custom-call(bf16[384,2048]{1,0:T(8,128)(2,1)} %bitcast.118, f32[384,1]{1,0:T(8,128)S(1)} %reshape.167.refs_1_, bf16[2048,256]{1,0:T(8,128)(2,1)} %bitcast.11.refs_2_, bf16[2048,256]{1,0:T(8,128)(2,1)} %bitcast.7.refs_3_, bf16[128,2048]{1,0:T(8,128)(2,1)S(1)} %get-tuple-element.211.refs_4_, ...), custom_call_target="tpu_custom_call" | custom-call | flops 4831838208 | bytes 12000000 | tf_op jit(solution)/shard_map/pallas_call | solution.py:512
  152.2 28.4 %shard_map.158 = bf16[48,2048]{1,0:T(8,128)(2,1)S(1)} custom-call(bf16[8,48,2048]{2,1,0:T(8,128)(2,1)S(1)} %bitcast.116, bf16[4,48,2048]{2,1,0:T(8,128)(2,1)S(1)} %bitcast.115, bf16[48,2048]{1,0:T(8,128)(2,1)S(1)} %constant_dynamic-slice_fusion.1.stream_ref), custom_call_target="tpu_custom_call" | custom-call | bytes 60000000 | tf_op jit(solution)/shard_map/pallas_call | solution.py:451
  180.6 0.7 copy.73
  (73 shorter events, 1.3 us)
Async XLA Ops:
  0.0 134.8 %copy-start = (bf16[256,2048]{1,0:T(8,128)(2,1)S(1)}, bf16[256,2048]{1,0:T(8,128)(2,1)}, u32[]{:S(2)}) copy-start(bf16[256,2048]{1,0:T(8,128)(2,1)} %param.33) | copy-start | bytes 3145732
  0.0 5.0 %copy-start.9 = (bf16[192,256]{1,0:T(8,128)(2,1)S(1)}, bf16[192,256]{1,0:T(8,128)(2,1)}, u32[]{:S(2)}) copy-start(bf16[192,256]{1,0:T(8,128)(2,1)} %param.18) | copy-start | bytes 294916
  0.0 5.1 %copy-start.2 = (bf16[192,128]{1,0:T(8,128)(2,1)S(1)}, bf16[192,128]{1,0:T(8,128)(2,1)}, u32[]{:S(2)}) copy-start(bf16[192,128]{1,0:T(8,128)(2,1)} %refs_1_.1) | copy-start | bytes 147460
  0.0 5.1 %copy-start.1 = (bf16[192,128]{1,0:T(8,128)(2,1)S(1)}, bf16[192,128]{1,0:T(8,128)(2,1)}, u32[]{:S(2)}) copy-start(bf16[192,128]{1,0:T(8,128)(2,1)} %refs_0_.1) | copy-start | bytes 147460
  0.0 42.1 %collective-permute-start = (bf16[48,2048]{1,0:T(8,128)(2,1)}, bf16[48,2048]{1,0:T(8,128)(2,1)}, u32[]{:S(2)}, u32[]{:S(2)}) collective-permute-start(bf16[48,2048]{1,0:T(8,128)(2,1)} %param.24), channel_id=1, source_target_pairs={{0,2},{1,3},{2,0},{3,1},{4,6},{5,7},{6,4},{7,5},{8,10},{9,11},{10,... | collective-permute-start | bytes 589832 | tf_op jit(solution)/shard_map/ppermute | solution.py:558
  3.1 40.2 %collective-permute-start.2 = (bf16[48,2048]{1,0:T(8,128)(2,1)}, bf16[48,2048]{1,0:T(8,128)(2,1)}, u32[]{:S(2)}, u32[]{:S(2)}) collective-permute-start(bf16[48,2048]{1,0:T(8,128)(2,1)} %param.24), channel_id=1, source_target_pairs={{0,1},{1,0},{2,3},{3,2},{4,5},{5,4},{6,7},{7,6},{8,9},{9,8},{10,11... | collective-permute-start | bytes 589832 | tf_op jit(solution)/shard_map/ppermute | solution.py:558
  4.4 52.7 %collective-permute-start.9 = (bf16[128,2048]{1,0:T(8,128)(2,1)S(1)}, bf16[128,2048]{1,0:T(8,128)(2,1)}, u32[]{:S(2)}, u32[]{:S(2)}) collective-permute-start(bf16[128,2048]{1,0:T(8,128)(2,1)S(1)} %get-tuple-element.211.refs_4_), channel_id=1, source_target_pairs={{0,2},{1,3},{2,0},{3,1},{4,6},{5,7},{6,4},{7,5},{8,10},{9,11},{10,... | collective-permute-start | bytes 1572872 | tf_op jit(solution)/shard_map/ppermute | solution.py:558
  4.6 53.0 %collective-permute-start.5 = (bf16[128,2048]{1,0:T(8,128)(2,1)S(1)}, bf16[128,2048]{1,0:T(8,128)(2,1)}, u32[]{:S(2)}, u32[]{:S(2)}) collective-permute-start(bf16[128,2048]{1,0:T(8,128)(2,1)S(1)} %get-tuple-element.211.refs_4_), channel_id=1, source_target_pairs={{0,1},{1,0},{2,3},{3,2},{4,5},{5,4},{6,7},{7,6},{8,9},{9,8},{10,11... | collective-permute-start | bytes 1572872 | tf_op jit(solution)/shard_map/ppermute | solution.py:558
  23.7 10.4 %copy-start.12 = (f32[2]{0:T(128)S(1)}, f32[2]{0:T(128)}, u32[]{:S(2)}) copy-start(f32[2]{0:T(128)} %param.21) | copy-start | bytes 28
  23.7 10.7 %copy-start.14 = (f32[128]{0:T(128)S(1)}, f32[128]{0:T(128)}, u32[]{:S(2)}) copy-start(f32[128]{0:T(128)} %param.22) | copy-start | bytes 1540
  33.9 8.1 %copy-start.13 = (s32[192,4]{0,1:T(4,128)S(1)}, s32[192,4]{0,1:T(4,128)}, u32[]{:S(2)}) copy-start(s32[192,4]{0,1:T(4,128)} %param.26) | copy-start | bytes 9220
  33.9 8.2 %copy-start.11 = (f32[48,4]{0,1:T(4,128)S(1)}, f32[48,4]{0,1:T(4,128)}, u32[]{:S(2)}) copy-start(f32[48,4]{0,1:T(4,128)} %param.27) | copy-start | bytes 2308
  41.0 14.9 %collective-permute-start.10 = (bf16[128,2048]{1,0:T(8,128)(2,1)S(1)}, bf16[128,2048]{1,0:T(8,128)(2,1)S(1)}, u32[]{:S(2)}, u32[]{:S(2)}) collective-permute-start(bf16[128,2048]{1,0:T(8,128)(2,1)S(1)} %get-tuple-element.145.refs_5_), channel_id=1, source_target_pairs={{0,2},{1,3},{2,0},{3,1},{4,6},{5,7},{6,4},{7,5},{8,10},{9,11},{10,... | collective-permute-start | bytes 1572872 | tf_op jit(solution)/shard_map/ppermute | solution.py:558
  42.1 36.3 %collective-permute-start.8 = (bf16[2048,256]{1,0:T(8,128)(2,1)}, bf16[2048,256]{1,0:T(8,128)(2,1)}, u32[]{:S(2)}, u32[]{:S(2)}) collective-permute-start(bf16[2048,256]{1,0:T(8,128)(2,1)} %bitcast.7.refs_3_), channel_id=1, source_target_pairs={{0,2},{1,3},{2,0},{3,1},{4,6},{5,7},{6,4},{7,5},{8,10},{9,11},{10,... | collective-permute-start | bytes 3145736 | tf_op jit(solution)/shard_map/ppermute | solution.py:558
  43.3 1.7 collective-permute-start.1
  45.0 55.8 %collective-permute-start.7 = (bf16[2048,256]{1,0:T(8,128)(2,1)}, bf16[2048,256]{1,0:T(8,128)(2,1)}, u32[]{:S(2)}, u32[]{:S(2)}) collective-permute-start(bf16[2048,256]{1,0:T(8,128)(2,1)} %bitcast.11.refs_2_), channel_id=1, source_target_pairs={{0,2},{1,3},{2,0},{3,1},{4,6},{5,7},{6,4},{7,5},{8,10},{9,11},{10,... | collective-permute-start | bytes 3145736 | tf_op jit(solution)/shard_map/ppermute | solution.py:558
  47.6 8.4 %copy-start.10 = (f32[2048]{0:T(1024)S(1)}, f32[2048]{0:T(1024)}, u32[]{:S(2)}) copy-start(f32[2048]{0:T(1024)} %param.25) | copy-start | bytes 24580
  51.0 80.8 %copy-start.8 = (bf16[192,2048]{1,0:T(8,128)(2,1)}, bf16[192,2048]{1,0:T(8,128)(2,1)S(1)}, u32[]{:S(2)}) copy-start(bf16[192,2048]{1,0:T(8,128)(2,1)S(1)} %get-tuple-element.214) | copy-start | bytes 2359300
  55.9 77.8 %copy-start.4 = (bf16[128,2048]{1,0:T(8,128)(2,1)}, bf16[128,2048]{1,0:T(8,128)(2,1)S(1)}, u32[]{:S(2)}) copy-start(bf16[128,2048]{1,0:T(8,128)(2,1)S(1)} %collective-permute-done.10.refs_13_) | copy-start | bytes 1572868
  55.9 1.9 %collective-permute-start.6 = (bf16[128,2048]{1,0:T(8,128)(2,1)S(1)}, bf16[128,2048]{1,0:T(8,128)(2,1)S(1)}, u32[]{:S(2)}, u32[]{:S(2)}) collective-permute-start(bf16[128,2048]{1,0:T(8,128)(2,1)S(1)} %get-tuple-element.145.refs_5_), channel_id=1, source_target_pairs={{0,1},{1,0},{2,3},{3,2},{4,5},{5,4},{6,7},{7,6},{8,9},{9,8},{10,11... | collective-permute-start | bytes 1572872 | tf_op jit(solution)/shard_map/ppermute | solution.py:558
  57.1 80.2 %collective-permute-start.3 = (bf16[2048,256]{1,0:T(8,128)(2,1)}, bf16[2048,256]{1,0:T(8,128)(2,1)}, u32[]{:S(2)}, u32[]{:S(2)}) collective-permute-start(bf16[2048,256]{1,0:T(8,128)(2,1)} %bitcast.11.refs_2_), channel_id=1, source_target_pairs={{0,1},{1,0},{2,3},{3,2},{4,5},{5,4},{6,7},{7,6},{8,9},{9,8},{10,11... | collective-permute-start | bytes 3145736 | tf_op jit(solution)/shard_map/ppermute | solution.py:558
  57.6 79.7 %collective-permute-start.4 = (bf16[2048,256]{1,0:T(8,128)(2,1)}, bf16[2048,256]{1,0:T(8,128)(2,1)}, u32[]{:S(2)}, u32[]{:S(2)}) collective-permute-start(bf16[2048,256]{1,0:T(8,128)(2,1)} %bitcast.7.refs_3_), channel_id=1, source_target_pairs={{0,1},{1,0},{2,3},{3,2},{4,5},{5,4},{6,7},{7,6},{8,9},{9,8},{10,11... | collective-permute-start | bytes 3145736 | tf_op jit(solution)/shard_map/ppermute | solution.py:558
  57.8 0.8 copy-start.6
  58.6 75.1 %collective-permute-start.14 = (bf16[128,2048]{1,0:T(8,128)(2,1)S(1)}, bf16[128,2048]{1,0:T(8,128)(2,1)}, u32[]{:S(2)}, u32[]{:S(2)}) collective-permute-start(bf16[128,2048]{1,0:T(8,128)(2,1)S(1)} %collective-permute-done.10.refs_13_), channel_id=1, source_target_pairs={{0,1},{1,0},{2,3},{3,2},{4,5},{5,4},{6,7},{7,6},{8,9},{9,8},{10,11... | collective-permute-start | bytes 1572872 | tf_op jit(solution)/shard_map/ppermute | solution.py:558
  78.5 58.9 %collective-permute-start.12 = (bf16[2048,256]{1,0:T(8,128)(2,1)}, bf16[2048,256]{1,0:T(8,128)(2,1)}, u32[]{:S(2)}, u32[]{:S(2)}) collective-permute-start(bf16[2048,256]{1,0:T(8,128)(2,1)} %collective-permute-done.8.refs_11_), channel_id=1, source_target_pairs={{0,1},{1,0},{2,3},{3,2},{4,5},{5,4},{6,7},{7,6},{8,9},{9,8},{10,11... | collective-permute-start | bytes 3145736 | tf_op jit(solution)/shard_map/ppermute | solution.py:558
  100.8 36.6 %collective-permute-start.11 = (bf16[2048,256]{1,0:T(8,128)(2,1)}, bf16[2048,256]{1,0:T(8,128)(2,1)}, u32[]{:S(2)}, u32[]{:S(2)}) collective-permute-start(bf16[2048,256]{1,0:T(8,128)(2,1)} %collective-permute-done.7.refs_10_), channel_id=1, source_target_pairs={{0,1},{1,0},{2,3},{3,2},{4,5},{5,4},{6,7},{7,6},{8,9},{9,8},{10,11... | collective-permute-start | bytes 3145736 | tf_op jit(solution)/shard_map/ppermute | solution.py:558
  130.6 1.2 copy-start.3
  133.8 3.5 %collective-permute-start.13 = (bf16[128,2048]{1,0:T(8,128)(2,1)}, bf16[128,2048]{1,0:T(8,128)(2,1)}, u32[]{:S(2)}, u32[]{:S(2)}) collective-permute-start(bf16[128,2048]{1,0:T(8,128)(2,1)} %collective-permute-done.9.refs_12_), channel_id=1, source_target_pairs={{0,1},{1,0},{2,3},{3,2},{4,5},{5,4},{6,7},{7,6},{8,9},{9,8},{10,11... | collective-permute-start | bytes 1572872 | tf_op jit(solution)/shard_map/ppermute | solution.py:558
  137.4 1.0 copy-start.5
  138.4 1.0 copy-start.7
